TPU v7x, 32 devices: a whole 2x2x4 slice. The times are simulated.
32 devices in a mesh: sp: 8 (over z, y), tp: 4 (over x, core).
Axes of the slice: x: 2, y: 2, z: 4, core: 2. Of those that a mesh axis runs over, the one named last changes fastest.
Arguments:
- tokens: bfloat16 [1280, 2048], P('sp'), may hold values from -6 to 6
- input_gain: float32 [2048], replicated, may hold values from 0.1 to 1.9
- chain_query: bfloat16 [2048, 1024], P('sp', 'tp'), may hold values from -0.125 to 0.125
- forward_gate: bfloat16 [2048, 1024], P('sp', 'tp'), may hold values from -0.125 to 0.125
- backward_gate: bfloat16 [2048, 1024], P('sp', 'tp'), may hold values from -0.125 to 0.125
- chain_value: bfloat16 [2048, 1024], P('sp', 'tp'), may hold values from -0.125 to 0.125
- output_gate: bfloat16 [2048, 1024], P('sp', 'tp'), may hold values from -0.125 to 0.125
- forget_rate: float32 [2, 1024], P(None, 'tp'), may hold values from 0.2 to 6
- chain_gain: float32 [1024], P('tp'), may hold values from 0.1 to 1.9
- query_down: bfloat16 [2048, 768], P('sp'), may hold values from -0.125 to 0.125
- latent_down: bfloat16 [2048, 512], P('sp'), may hold values from -0.125 to 0.125
- rotary_down: bfloat16 [2048, 64], replicated, may hold values from -0.125 to 0.125
- query_latent_gain: float32 [768], replicated, may hold values from 0.1 to 1.9
- latent_gain: float32 [512], replicated, may hold values from 0.1 to 1.9
- query_up: bfloat16 [768, 1536], P(None, 'tp'), may hold values from -0.21875 to 0.21875
- latent_up: bfloat16 [512, 2048], P(None, 'tp'), may hold values from -0.25 to 0.25
- query_head_gain: float32 [192], replicated, may hold values from 0.1 to 1.9
- key_head_gain: float32 [192], replicated, may hold values from 0.1 to 1.9
- mixer_gain: float32 [1024], P('tp'), may hold values from 0.1 to 1.9
- chain_out: bfloat16 [1024, 2048], P('tp', 'sp'), may hold values from -0.125 to 0.125
- attend_out: bfloat16 [1024, 2048], P('tp', 'sp'), may hold values from -0.125 to 0.125
Outputs:
- mixed: float32 [1280, 2048], P(('sp', 'tp'))
All inputs are finite; a program needn't handle non-finite values.
Results may differ from a plain program's by a relative error of at most 0.017.
Values may be sent and summed in bfloat16 or wider, within the bound.
A program may use at most 128 MiB of HBM per device.

v0:
```python
import jax
import jax.numpy as jnp
from jax import lax
from jax.sharding import PartitionSpec as P

KEY_DIM = 128
VAL_DIM = 128
NOPE_DIM = 128
ROPE_DIM = 64
VHEAD_DIM = 128
ATT_QK = 192


norm_eps = 1e-06
rope_theta = 10000.0
finest_arithmetic_mode = lax.Precision.HIGHEST


def entering(value, axis, combine, identity, reverse):
    count, position = (lax.axis_size(axis), lax.axis_index(axis))
    everything = jax.tree.map(lambda part: lax.all_gather(part, axis), value)
    start = jax.tree.map(
        lambda part, zero: jnp.broadcast_to(jnp.asarray(zero, part.dtype), part.shape),
        value,
        identity,
    )

    def step(k, before):
        at = count - 1 - k if reverse else k
        reached = at > position if reverse else at < position
        new = combine(before, jax.tree.map(lambda part: part[at], everything))
        return jax.tree.map(lambda a, b: jnp.where(reached, a, b), new, before)

    return lax.fori_loop(0, count, step, start)


def rms_scale(values, gain_vec):
    mean_square = jnp.mean(values * values, axis=-1, keepdims=True)
    return values * lax.rsqrt(mean_square + norm_eps) * gain_vec


def rotate_tail(values, positions):
    half_dim = ROPE_DIM // 2
    inverse = rope_theta ** (-jnp.arange(0, ROPE_DIM, 2).astype(jnp.float32) / ROPE_DIM)
    angles = positions.astype(jnp.float32)[:, None] * inverse
    cosine = jnp.cos(angles)[:, None, :]
    sine_table = jnp.sin(angles)[:, None, :]
    unrotated = values[..., :NOPE_DIM]
    first_half = values[..., NOPE_DIM : NOPE_DIM + half_dim]
    latter_element = values[..., NOPE_DIM + half_dim :]
    return jnp.concatenate(
        [
            unrotated,
            first_half * cosine - latter_element * sine_table,
            latter_element * cosine + first_half * sine_table,
        ],
        axis=-1,
    )


def gate_parts(pre_gate, rate_row, seq_len):
    opening = rate_row / seq_len * jax.nn.sigmoid(-pre_gate.astype(jnp.float32))
    return (jnp.log1p(-opening), opening)


def summarize(query_rows, key_rows, payload_array_lines, log_decay):
    cumulative = jnp.cumsum(log_decay, axis=0)
    weighted_probe_vectors = query_rows * jnp.exp(cumulative)
    weighted_lookup_vectors = key_rows * jnp.exp(-cumulative)
    overall_shrink_multiplier = jnp.exp(cumulative[-1])
    recurrent_memory_digest = overall_shrink_multiplier[:, :, None] * jnp.einsum(
        "jre,jrw->rew",
        weighted_lookup_vectors,
        payload_array_lines,
        precision=finest_arithmetic_mode,
    )
    return (
        weighted_probe_vectors,
        weighted_lookup_vectors,
        overall_shrink_multiplier,
        recurrent_memory_digest,
    )


def emit(weighted_probe_vectors, weighted_lookup_vectors, payload_array_lines, incoming_update):
    length = weighted_probe_vectors.shape[0]
    lower_mask = jnp.tril(jnp.ones((length, length), jnp.float32))
    scores = (
        jnp.einsum(
            "thk,shk->hts",
            weighted_probe_vectors,
            weighted_lookup_vectors,
            precision=finest_arithmetic_mode,
        )
        * lower_mask
    )
    within = jnp.einsum(
        "hts,shv->thv", scores, payload_array_lines, precision=finest_arithmetic_mode
    )
    prior_state = jnp.einsum(
        "mjf,jfi->mji", weighted_probe_vectors, incoming_update, precision=finest_arithmetic_mode
    )
    return within + prior_state


def chain_combine(earlier, following):
    return (earlier[0] * following[0], following[0][:, :, None] * earlier[1] + following[1])


def add_scores(running, query_final, key_piece, value_piece):
    score_scale = query_final.shape[-1] ** (-0.5)
    scores = (
        jnp.einsum("qhd,khd->hqk", query_final, key_piece, preferred_element_type=jnp.float32)
        * score_scale
    )
    weights = jnp.exp(scores)
    numerator = running[0] + jnp.einsum(
        "hqk,khv->qhv",
        weights.astype(jnp.bfloat16),
        value_piece,
        preferred_element_type=jnp.float32,
    )
    return (numerator, running[1] + jnp.sum(weights, axis=-1))


def on_device(
    tokens,
    input_gain,
    chain_query,
    forward_gate,
    backward_gate,
    chain_value,
    output_gate,
    forget_rate,
    chain_gain,
    query_down,
    latent_down,
    rotary_down,
    query_latent_gain,
    latent_gain,
    query_up,
    latent_up,
    query_head_gain,
    key_head_gain,
    mixer_gain,
    chain_out,
    attend_out,
):
    query_cols = query_down.shape[1] // lax.axis_size("tp")
    latent_cols = latent_down.shape[1] // lax.axis_size("tp")
    query_source = lax.dynamic_slice_in_dim(
        query_down, lax.axis_index("tp") * query_cols, query_cols, 1
    )
    latent_source = lax.dynamic_slice_in_dim(
        latent_down, lax.axis_index("tp") * latent_cols, latent_cols, 1
    )
    gathered = (
        lax.all_gather(chain_query, "sp", axis=0, tiled=True),
        lax.all_gather(forward_gate, "sp", axis=0, tiled=True),
        lax.all_gather(backward_gate, "sp", axis=0, tiled=True),
        lax.all_gather(chain_value, "sp", axis=0, tiled=True),
        lax.all_gather(output_gate, "sp", axis=0, tiled=True),
        lax.all_gather(query_source, "sp", axis=0, tiled=True),
        lax.all_gather(latent_source, "sp", axis=0, tiled=True),
        lax.all_gather(chain_out, "sp", axis=1, tiled=True),
        lax.all_gather(attend_out, "sp", axis=1, tiled=True),
    )
    (
        full_query,
        full_forward,
        full_backward,
        full_value,
        full_outgate,
        full_query_down,
        full_latent_down,
        full_chain_out,
        full_attend_out,
    ) = gathered
    tok_rows = tokens.shape[0]
    seq_len = tok_rows * lax.axis_size("sp")
    normed = rms_scale(tokens.astype(jnp.float32), input_gain).astype(jnp.bfloat16)

    def project(source, weight):
        return jnp.dot(source, weight, preferred_element_type=jnp.float32).astype(jnp.bfloat16)

    def heads_of(tensor, head_width):
        return tensor.astype(jnp.float32).reshape(
            tok_rows, tensor.shape[1] // head_width, head_width
        )

    def row_term(source, weight):
        return jnp.dot(source, weight, preferred_element_type=jnp.float32)

    query_rows = heads_of(project(normed, full_query), KEY_DIM)
    payload_array_lines = heads_of(project(normed, full_value), VAL_DIM)
    forward_log, forward_key = gate_parts(project(normed, full_forward), forget_rate[0], seq_len)
    backward_log, backward_key = gate_parts(project(normed, full_backward), forget_rate[1], seq_len)
    gate_logit = project(normed, full_outgate).astype(jnp.float32)
    chain_heads = query_rows.shape[1]
    identity = (
        jnp.ones((chain_heads, KEY_DIM), jnp.float32),
        jnp.zeros((chain_heads, KEY_DIM, VAL_DIM), jnp.float32),
    )
    forward_parts = summarize(
        query_rows,
        heads_of(forward_key, KEY_DIM),
        payload_array_lines,
        heads_of(forward_log, KEY_DIM),
    )
    forward_in = entering(
        (forward_parts[2], forward_parts[3]), "sp", chain_combine, identity, False
    )[1]
    flipped_values = jnp.flip(payload_array_lines, 0)
    backward_parts = summarize(
        jnp.flip(query_rows, 0),
        jnp.flip(heads_of(backward_key, KEY_DIM), 0),
        flipped_values,
        jnp.flip(heads_of(backward_log, KEY_DIM), 0),
    )
    backward_in = entering(
        (backward_parts[2], backward_parts[3]), "sp", chain_combine, identity, True
    )[1]
    combined = emit(forward_parts[0], forward_parts[1], payload_array_lines, forward_in) + jnp.flip(
        emit(backward_parts[0], backward_parts[1], flipped_values, backward_in), 0
    )
    head_gain = chain_gain.reshape(chain_heads, VAL_DIM)
    chain_mixed = (
        rms_scale(combined, head_gain).reshape(tok_rows, -1) * jax.nn.silu(gate_logit)
    ).astype(jnp.bfloat16)
    raw_query_latent = project(normed, full_query_down)
    raw_pair_latent = project(normed, full_latent_down)
    raw_query_latent, raw_pair_latent = (
        lax.all_gather(raw_query_latent, "tp", axis=1, tiled=True),
        lax.all_gather(raw_pair_latent, "tp", axis=1, tiled=True),
    )
    query_latent = rms_scale(raw_query_latent.astype(jnp.float32), query_latent_gain).astype(
        jnp.bfloat16
    )
    pair_latent = rms_scale(raw_pair_latent.astype(jnp.float32), latent_gain).astype(jnp.bfloat16)
    rotary_key = project(normed, rotary_down).astype(jnp.float32)
    attend_heads = query_up.shape[1] // ATT_QK
    attend_query = (
        project(query_latent, query_up).astype(jnp.float32).reshape(tok_rows, attend_heads, ATT_QK)
    )
    attend_pairs = project(pair_latent, latent_up).reshape(
        tok_rows, attend_heads, NOPE_DIM + VHEAD_DIM
    )
    positions = lax.axis_index("sp") * tok_rows + jnp.arange(tok_rows, dtype=jnp.int32)
    query_final = rotate_tail(rms_scale(attend_query, query_head_gain), positions).astype(
        jnp.bfloat16
    )
    key_cat = jnp.concatenate(
        [
            attend_pairs[..., :NOPE_DIM].astype(jnp.float32),
            jnp.broadcast_to(rotary_key[:, None, :], (tok_rows, attend_heads, ROPE_DIM)),
        ],
        axis=-1,
    )
    key_final = rotate_tail(rms_scale(key_cat, key_head_gain), positions).astype(jnp.bfloat16)
    keys_flat = key_final.reshape(tok_rows, attend_heads * ATT_QK)
    values_flat = attend_pairs[..., NOPE_DIM:].reshape(tok_rows, attend_heads * VHEAD_DIM)

    def fold_keys(running, pieces):
        key_piece = pieces[0].reshape(pieces[0].shape[0], attend_heads, ATT_QK)
        value_piece = pieces[1].reshape(pieces[1].shape[0], attend_heads, VHEAD_DIM)
        piece_rows = key_piece.shape[0]
        span_rows = 1024
        if piece_rows > span_rows and piece_rows % span_rows == 0:

            def one_span(partial_sum, interval_couple):
                return (
                    add_scores(partial_sum, query_final, interval_couple[0], interval_couple[1]),
                    None,
                )

            shaped = (
                key_piece.reshape(piece_rows // span_rows, span_rows, attend_heads, ATT_QK),
                value_piece.reshape(piece_rows // span_rows, span_rows, attend_heads, VHEAD_DIM),
            )
            result, _ = lax.scan(one_span, running, shaped)
            return result
        return add_scores(running, query_final, key_piece, value_piece)

    start_sum = (
        jnp.zeros((tok_rows, attend_heads, VHEAD_DIM), jnp.float32),
        jnp.zeros((attend_heads, tok_rows), jnp.float32),
    )
    numerator, denominator = fold_keys(
        start_sum,
        (
            lax.all_gather(keys_flat, "sp", axis=0, tiled=True),
            lax.all_gather(values_flat, "sp", axis=0, tiled=True),
        ),
    )
    attend_rows = numerator / jnp.transpose(denominator)[:, :, None]
    attend_mixed = (
        rms_scale(attend_rows, mixer_gain.reshape(attend_heads, VHEAD_DIM))
        .reshape(tok_rows, attend_heads * VHEAD_DIM)
        .astype(jnp.bfloat16)
    )
    return lax.psum_scatter(
        row_term(chain_mixed, full_chain_out) + row_term(attend_mixed, full_attend_out),
        "tp",
        scatter_dimension=0,
        tiled=True,
    )


def solution(mesh):
    placed = (
        P("sp", None),
        P(),
        P("sp", "tp"),
        P("sp", "tp"),
        P("sp", "tp"),
        P("sp", "tp"),
        P("sp", "tp"),
        P(None, "tp"),
        P("tp"),
        P("sp", None),
        P("sp", None),
        P(),
        P(),
        P(),
        P(None, "tp"),
        P(None, "tp"),
        P(),
        P(),
        P("tp"),
        P("tp", "sp"),
        P("tp", "sp"),
    )
    return jax.shard_map(
        on_device, mesh=mesh, in_specs=placed, out_specs=P(("sp", "tp"), None), check_vma=False
    )
```

profile of v0, /device:TPU:1, one launch (start us, length us, event | category | flops | bytes accessed | tf_op | source)
XLA Modules:
  0.0 427.8 jit_solution(1413293845524159147)
XLA Ops:
  9.4 1.3 fusion.3
  11.4 38.7 %all-gather.19.cloned.1.call-done = bf16[2048,256]{1,0:T(8,128)(2,1)} async-done(((bf16[256,256]{1,0:T(8,128)(2,1)}), bf16[2048,256]{1,0:T(8,128)(2,1)}) %all-gather.19.cloned.1.call-update) | async-done | bytes 1048592 | tf_op jit(solution)/shard_map/all_gather | solution.py:160
  50.1 1.8 fusion.16
  53.2 38.1 %all-gather.13.cloned.1.call-done = bf16[2048,256]{1,0:T(8,128)(2,1)} async-done(((bf16[256,256]{1,0:T(8,128)(2,1)}), bf16[2048,256]{1,0:T(8,128)(2,1)}) %all-gather.13.cloned.1.call-update) | async-done | bytes 1048592 | tf_op jit(solution)/shard_map/all_gather | solution.py:161
  91.3 1.6 fusion.24
  93.3 1.3 convolution_multiply_fusion.3
  94.7 37.8 %all-gather.17.cloned.1.call-done = bf16[2048,256]{1,0:T(8,128)(2,1)} async-done(((bf16[256,256]{1,0:T(8,128)(2,1)}), bf16[2048,256]{1,0:T(8,128)(2,1)}) %all-gather.17.cloned.1.call-update) | async-done | bytes 1048592 | tf_op jit(solution)/shard_map/all_gather | solution.py:159
  132.4 1.6 fusion.21
  134.6 1.1 convolution_multiply_fusion.4
  138.9 26.4 %all_gather.71 = bf16[2048,128]{1,0:T(8,128)(2,1)S(1)} all-gather(bf16[256,128]{1,0:T(8,128)(2,1)S(1)} %constant_dynamic-slice_fusion.1), channel_id=1, replica_groups=mesh['sp'=8,'tp'=4] {'sp'}, dimensions={0}, use_global_device_ids=true | all-gather | bytes 589824 | tf_op jit(solution)/shard_map/all_gather | solution.py:164
  165.7 13.4 %all_gather.72 = bf16[160,512]{1,0:T(8,128)(2,1)S(1)} all-gather(bf16[160,128]{1,0:T(8,128)(2,1)S(1)} %convolution_convert_fusion.8), channel_id=1, replica_groups=mesh['sp'=8,'tp'=4] {'tp'}, dimensions={1}, use_global_device_ids=true | all-gather | bytes 204800 | tf_op jit(solution)/shard_map/all_gather | solution.py:234
  180.4 1.4 fusion.26
  183.1 28.2 %all_gather.74 = bf16[2048,192]{1,0:T(8,128)(2,1)S(1)} all-gather(bf16[256,192]{1,0:T(8,128)(2,1)S(1)} %constant_dynamic-slice_fusion), channel_id=1, replica_groups=mesh['sp'=8,'tp'=4] {'sp'}, dimensions={0}, use_global_device_ids=true | all-gather | bytes 884736 | tf_op jit(solution)/shard_map/all_gather | solution.py:163
  211.8 12.4 %all-gather.2 = bf16[4,192,160]{1,2,0:T(8,128)(2,1)S(1)} all-gather(bf16[1,192,160]{1,2,0:T(8,128)(2,1)S(1)} %fusion.25), channel_id=1, replica_groups=mesh['sp'=8,'tp'=4] {'tp'}, dimensions={0}, use_global_device_ids=true | all-gather | bytes 307200 | tf_op jit(solution)/shard_map/all_gather | solution.py:233
  228.4 28.1 %all_gather.76 = bf16[1280,384]{1,0:T(8,128)(2,1)S(1)} all-gather(bf16[160,384]{1,0:T(8,128)(2,1)S(1)} %convert_element_type.124), channel_id=1, replica_groups=mesh['sp'=8,'tp'=4] {'sp'}, dimensions={0}, use_global_device_ids=true | all-gather | bytes 1105920 | tf_op jit(solution)/shard_map/all_gather | solution.py:291
  256.5 1.4 copy.110
  257.9 26.8 %all_gather.73 = bf16[1280,256]{1,0:T(8,128)(2,1)S(1)} all-gather(bf16[160,256]{1,0:T(8,128)(2,1)S(1)} %bitcast.170), channel_id=1, replica_groups=mesh['sp'=8,'tp'=4] {'sp'}, dimensions={0}, use_global_device_ids=true | all-gather | bytes 737280 | tf_op jit(solution)/shard_map/all_gather | solution.py:292
  284.7 1.1 copy.103
  285.9 1.8 fusion.75
  288.8 16.0 %all_gather.66 = f32[8,2,128]{2,1,0:T(2,128)S(1)} all-gather(f32[1,2,128]{2,1,0:T(2,128)S(1)} %bitcast.172), channel_id=1, replica_groups=mesh['sp'=8,'tp'=4] {'sp'}, dimensions={0}, use_global_device_ids=true | all-gather | bytes 9216 | tf_op jit(solution)/shard_map/all_gather | solution.py:21
  304.7 1.6 fusion.23
  307.8 13.2 %all_gather.62 = f32[8,2,128]{2,1,0:T(2,128)S(1)} all-gather(f32[1,2,128]{2,1,0:T(2,128)S(1)} %bitcast.174), channel_id=1, replica_groups=mesh['sp'=8,'tp'=4] {'sp'}, dimensions={0}, use_global_device_ids=true | all-gather | bytes 9216 | tf_op jit(solution)/shard_map/all_gather | solution.py:21
  321.0 8.7 %while.31 = (s32[]{:T(128)}, f32[2,128,128]{2,1,0:T(8,128)S(1)}, s32[]{:T(128)}, f32[8,2,128]{2,1,0:T(2,128)S(1)}, f32[8,2,128,128]{3,2,1,0:T(8,128)}, /*index=5*/s32[]{:T(128)}, s32[]{:T(128)}, s32[]{:T(128)}, s32[]{:T(128)}) while((s32[]{:T(128)}, f32[2,128,128]{2,1,0:T(8,128)S(1)}, s32[]{:T(128)}, f32[8,2,128]{2,1,0:T(2,128)S(1)}, ...), condition=%wide.region_8.9_spmd.clone, body=%wide.region_7.8_spmd.clone.sunk | while | flops 131080 | bytes 396455 | solution.py:34
  325.4 1.0 fusion.105
  329.7 8.7 %while.30 = (s32[]{:T(128)}, f32[2,128,128]{2,1,0:T(8,128)S(1)}, s32[]{:T(128)}, f32[8,2,128]{2,1,0:T(2,128)S(1)}, f32[8,2,128,128]{3,2,1,0:T(8,128)}, /*index=5*/s32[]{:T(128)}, s32[]{:T(128)}) while((s32[]{:T(128)}, f32[2,128,128]{2,1,0:T(8,128)S(1)}, s32[]{:T(128)}, f32[8,2,128]{2,1,0:T(2,128)S(1)}, ...), condition=%wide.region_4.5_spmd.clone, body=%wide.region_3.4_spmd.clone.sunk | while | flops 131076 | bytes 396393 | solution.py:34
  329.8 1.1 fusion.104
  330.9 1.0 fusion.104
  340.3 9.6 %all-gather.23.cloned.1.call-done = bf16[256,2048]{1,0:T(8,128)(2,1)} async-done(((bf16[256,256]{1,0:T(8,128)(2,1)}), bf16[256,2048]{1,0:T(8,128)(2,1)}) %all-gather.23.cloned.1.call-update) | async-done | bytes 1048592 | tf_op jit(solution)/shard_map/all_gather | solution.py:165
  349.9 2.5 fusion.51
  352.5 38.0 %all-gather.25.cloned.1.call-done = bf16[256,2048]{1,0:T(8,128)(2,1)} async-done(((bf16[256,256]{1,0:T(8,128)(2,1)}), bf16[256,2048]{1,0:T(8,128)(2,1)}) %all-gather.25.cloned.1.call-update) | async-done | bytes 1048592 | tf_op jit(solution)/shard_map/all_gather | solution.py:166
  390.4 2.7 convolution_add_fusion
  393.1 27.9 %reduce-scatter.2.cloned.1.call-done = f32[40,2048]{1,0:T(8,128)} async-done(((f32[160,2048]{1,0:T(8,128)}), f32[40,2048]{1,0:T(8,128)}) %reduce-scatter.2.cloned.1.call-update) | async-done | bytes 327696 | tf_op jit(solution)/shard_map/reduce_scatter | solution.py:301
  (179 shorter events, 33.9 us)
Async XLA Ops:
  6.5 218.5 %copy-start = (bf16[768,384]{1,0:T(8,128)(2,1)S(1)}, bf16[768,384]{1,0:T(8,128)(2,1)}, u32[]{:S(2)}) copy-start(bf16[768,384]{1,0:T(8,128)(2,1)} %param.39) | copy-start | bytes 1769476
  6.5 43.6 %all-gather.19.cloned.1.call-start = ((), (), s32[]{:S(2)}) async-start(), calls=%async_computation.4 | async-start | bytes 1179648 | tf_op jit(solution)/shard_map/all_gather | solution.py:160
  7.3 84.0 %all-gather.13.cloned.1.call-start = ((), (), s32[]{:S(2)}) async-start(), calls=%async_computation.1 | async-start | bytes 1179648 | tf_op jit(solution)/shard_map/all_gather | solution.py:161
  8.0 124.4 %all-gather.17.cloned.1.call-start = ((), (), s32[]{:S(2)}) async-start(), calls=%async_computation.3 | async-start | bytes 1179648 | tf_op jit(solution)/shard_map/all_gather | solution.py:159
  8.7 296.0 %all-gather.15.cloned.1.call-start = ((), (), s32[]{:S(2)}) async-start(), calls=%async_computation.2 | async-start | bytes 1179648 | tf_op jit(solution)/shard_map/all_gather | solution.py:158
  9.3 311.7 %all-gather.29.cloned.1.call-start = ((), (), s32[]{:S(2)}) async-start(), calls=%async_computation.10 | async-start | bytes 1179648 | tf_op jit(solution)/shard_map/all_gather | solution.py:21
  52.4 38.9 %copy-start.1 = (bf16[160,2048]{1,0:T(8,128)(2,1)S(1)}, bf16[160,2048]{1,0:T(8,128)(2,1)}, u32[]{:S(2)}) copy-start(bf16[160,2048]{1,0:T(8,128)(2,1)} %param.25) | copy-start | bytes 1966084
  52.4 38.9 %copy-start.19 = (f32[2048]{0:T(1024)S(1)}, f32[2048]{0:T(1024)}, u32[]{:S(2)}) copy-start(f32[2048]{0:T(1024)} %param.26) | copy-start | bytes 24580
  53.2 40.1 %copy-start.6 = (f32[160,2,128]{2,0,1:T(8,128)}, f32[160,2,128]{2,0,1:T(8,128)S(1)}, u32[]{:S(2)}) copy-start(f32[160,2,128]{2,0,1:T(8,128)S(1)} %rev.19) | copy-start | bytes 491524
  92.9 41.7 %copy-start.10 = (bf16[20,2,8,128]{3,2,1,0:T(8,128)(2,1)}, bf16[20,2,8,128]{3,2,1,0:T(8,128)(2,1)S(1)}, u32[]{:S(2)}) copy-start(bf16[20,2,8,128]{3,2,1,0:T(8,128)(2,1)S(1)} %fusion.24) | copy-start | bytes 245764
  93.3 40.8 %copy-start.8 = (f32[160,2,128]{2,0,1:T(8,128)}, f32[160,2,128]{2,0,1:T(8,128)S(1)}, u32[]{:S(2)}) copy-start(f32[160,2,128]{2,0,1:T(8,128)S(1)} %rev.16) | copy-start | bytes 491524
  94.6 235.1 %all-gather.27.cloned.1.call-start = ((), (), s32[]{:S(2)}) async-start(), calls=%async_computation.9 | async-start | bytes 1179648 | tf_op jit(solution)/shard_map/all_gather | solution.py:21
  135.7 204.6 %all-gather.21.cloned.1.call-start = ((), (), s32[]{:S(2)}) async-start(), calls=%async_computation.5 | async-start | bytes 1179648 | tf_op jit(solution)/shard_map/all_gather | solution.py:162
  136.4 213.5 %all-gather.23.cloned.1.call-start = ((), (), s32[]{:S(2)}) async-start(), calls=%async_computation.6 | async-start | bytes 1179648 | tf_op jit(solution)/shard_map/all_gather | solution.py:165
  137.2 253.2 %all-gather.25.cloned.1.call-start = ((), (), s32[]{:S(2)}) async-start(), calls=%async_computation.7 | async-start | bytes 1179648 | tf_op jit(solution)/shard_map/all_gather | solution.py:166
  137.9 283.1 %reduce-scatter.2.cloned.1.call-start = ((), (), s32[]{:S(2)}) async-start(), calls=%async_computation.8 | async-start | bytes 1638400 | tf_op jit(solution)/shard_map/reduce_scatter | solution.py:301
  138.9 40.3 %copy-start.13 = (bf16[512,512]{1,0:T(8,128)(2,1)S(1)}, bf16[512,512]{1,0:T(8,128)(2,1)}, u32[]{:S(2)}) copy-start(bf16[512,512]{1,0:T(8,128)(2,1)} %param.40) | copy-start | bytes 1572868
  138.9 40.4 %copy-start.21 = (f32[512]{0:T(512)S(1)}, f32[512]{0:T(512)}, u32[]{:S(2)}) copy-start(f32[512]{0:T(512)} %param.38) | copy-start | bytes 6148
  180.4 31.0 %copy-start.2 = (f32[160,2,128]{2,0,1:T(8,128)}, f32[160,2,128]{2,0,1:T(8,128)S(1)}, u32[]{:S(2)}) copy-start(f32[160,2,128]{2,0,1:T(8,128)S(1)} %copy_convert_fusion) | copy-start | bytes 491524
  181.9 29.9 %copy-start.4 = (f32[160,2,64]{2,0,1:T(8,128)}, f32[160,2,64]{2,0,1:T(8,128)S(1)}, u32[]{:S(2)}) copy-start(f32[160,2,64]{2,0,1:T(8,128)S(1)} %broadcast_in_dim.11) | copy-start | bytes 245764
  225.0 1.0 copy-start.3
  225.0 1.0 copy-start.5
  256.5 1.4 copy-start.14
  257.9 28.0 %copy-start.16 = (bf16[160,2,32]{2,0,1:T(8,128)(2,1)S(1)}, bf16[160,2,32]{2,0,1:T(8,128)(2,1)}, u32[]{:S(2)}) copy-start(bf16[160,2,32]{2,0,1:T(8,128)(2,1)} %get-tuple-element.299) | copy-start | bytes 61444
  257.9 28.0 %copy-start.17 = (bf16[160,2,32]{2,0,1:T(8,128)(2,1)S(1)}, bf16[160,2,32]{2,0,1:T(8,128)(2,1)}, u32[]{:S(2)}) copy-start(bf16[160,2,32]{2,0,1:T(8,128)(2,1)} %get-tuple-element.300) | copy-start | bytes 61444
  257.9 28.0 %copy-start.18 = (bf16[160,2,128]{2,0,1:T(8,128)(2,1)S(1)}, bf16[160,2,128]{2,0,1:T(8,128)(2,1)}, u32[]{:S(2)}) copy-start(bf16[160,2,128]{2,0,1:T(8,128)(2,1)} %slice.121) | copy-start | bytes 245764
  285.9 1.8 copy-start.12
  329.7 9.0 %copy-start.9 = (f32[160,2,128]{2,0,1:T(8,128)S(1)}, f32[160,2,128]{2,0,1:T(8,128)}, u32[]{:S(2)}) copy-start(f32[160,2,128]{2,0,1:T(8,128)} %copy-done.8) | copy-start | bytes 491524
  338.4 1.4 copy-start.11
  338.8 11.2 %copy-start.24 = (f32[256]{0:T(256)S(1)}, f32[256]{0:T(256)}, u32[]{:S(2)}) copy-start(f32[256]{0:T(256)} %param.33) | copy-start | bytes 3076
  349.9 40.5 %copy-start.15 = (f32[160,2,128]{2,0,1:T(8,128)S(1)}, f32[160,2,128]{2,0,1:T(8,128)}, u32[]{:S(2)}) copy-start(f32[160,2,128]{2,0,1:T(8,128)} %get-tuple-element.316) | copy-start | bytes 491524
  349.9 40.5 %copy-start.25 = (f32[256]{0:T(256)S(1)}, f32[256]{0:T(256)}, u32[]{:S(2)}) copy-start(f32[256]{0:T(256)} %param.43) | copy-start | bytes 3076
  (4 other events, 3.8 us)
Sparse Core Ops, SparseCore 0:
  9.5 40.6 all-gather.18
  52.3 38.9 all-gather.12
  93.4 38.9 all-gather.16
  134.4 40.8 all-gather.14
  177.3 45.3 all-gather.28
  224.6 44.5 all-gather.26
  271.3 39.3 all-gather.20
  312.7 37.1 all-gather.22
  352.0 38.4 all-gather.24
  393.2 27.7 reduce-scatter.1
where the time goes:
time: 430 us; the launch traced here: 428 us
  waiting for transfers between devices  195 us (45%)
  blocking collectives  165 us (38%)
  matrix products  22.4 us (5%)
  other arithmetic  21.7 us (5%)
  between operations  14.3 us (3%)
  local copies, waits for them, and re-layouts  9.24 us (2%)
    all_gather x1, waiting for transfers between devices, on_device(): lax.all_gather(backward_gate, 'sp', axis=0, tiled=True)  38.7 us
    all_gather x1, waiting for transfers between devices, on_device(): lax.all_gather(chain_value, 'sp', axis=0, tiled=True)  38.1 us
    all_gather x1, waiting for transfers between devices, on_device(): lax.all_gather(attend_out, 'sp', axis=1, tiled=True)  38 us
    all_gather x1, waiting for transfers between devices, on_device(): lax.all_gather(forward_gate, 'sp', axis=0, tiled=True)  37.8 us
    all_gather x2, blocking collectives, entering(): everything = jax.tree.map(lambda part: lax.all_gather(part, axis), value)  29.2 us
    all_gather x1, blocking collectives, on_device(): lax.all_gather(query_source, 'sp', axis=0, tiled=True)  28.2 us
    all_gather x1, blocking collectives, on_device(): lax.all_gather(keys_flat, 'sp', axis=0, tiled=True)  28.1 us
    reduce_scatter x1, waiting for transfers between devices, on_device(): lax.psum_scatter(row_term(chain_mixed, full_chain_out) + row_term(attend_...  27.9 us
  transfers between devices with their start and end apart: 10, of which 6 were waited for; matrix products, arithmetic and copies ran while one was open for 12% of the time, Pallas kernels for 0%

commit v1 on v0

v1 whole, which is shorter than its diff:
```python
import functools

import jax
import jax.numpy as jnp
from jax import lax
from jax.experimental import pallas as pl
from jax.experimental.pallas import tpu as pltpu
from jax.sharding import PartitionSpec as P

KEY_DIM = 128
VAL_DIM = 128
NOPE_DIM = 128
ROPE_DIM = 64
VHEAD_DIM = 128
ATT_QK = 192

norm_eps = 1e-06
rope_theta = 10000.0
MESH = pl.DeviceIdType.MESH
VMEM_LIMIT = 60 * 1024 * 1024
f32 = jnp.float32
bf16 = jnp.bfloat16


def rms_scale(values, gain_vec):
    mean_square = jnp.mean(values * values, axis=-1, keepdims=True)
    return values * lax.rsqrt(mean_square + norm_eps) * gain_vec


def rotate_tail(values, positions):
    half_dim = ROPE_DIM // 2
    inverse = rope_theta ** (-jnp.arange(0, ROPE_DIM, 2).astype(f32) / ROPE_DIM)
    angles = positions.astype(f32)[:, None] * inverse
    cosine = jnp.cos(angles)[:, None, :]
    sine_table = jnp.sin(angles)[:, None, :]
    unrotated = values[..., :NOPE_DIM]
    first_half = values[..., NOPE_DIM : NOPE_DIM + half_dim]
    latter = values[..., NOPE_DIM + half_dim :]
    return jnp.concatenate(
        [
            unrotated,
            first_half * cosine - latter * sine_table,
            latter * cosine + first_half * sine_table,
        ],
        axis=-1,
    )


def greet(peers):
    barrier = pltpu.get_barrier_semaphore()
    for peer in peers:
        pl.semaphore_signal(barrier, inc=1, device_id=peer, device_id_type=MESH)
    pl.semaphore_wait(barrier, len(peers))


def line_and_pair(n):
    me = lax.axis_index("sp")
    lines = n // 2
    outer, inner = me // 2, lax.rem(me, 2)
    partner = {"sp": outer * 2 + 1 - inner}

    def line_peer(d):
        return {"sp": lax.rem(outer + d, lines) * 2 + inner}

    return me, lines, outer, inner, partner, line_peer


def project_kernel(n, count, x_ref, *refs):
    weights = refs[:count]
    outs = refs[count : 2 * count]
    rest = refs[2 * count :]
    x_recv = rest[0]
    w_recv = rest[1 : 1 + count]
    p_send = rest[1 + count : 1 + 2 * count]
    p_recv = rest[1 + 2 * count : 1 + 3 * count]
    own = rest[1 + 3 * count : 1 + 4 * count]
    xs, xr, ws, wr, ps, pr = rest[1 + 4 * count :]
    me, lines, outer, inner, partner, line_peer = line_and_pair(n)
    greet([partner] + [line_peer(d) for d in range(1, lines)])

    def w_copy(c):
        return pltpu.make_async_remote_copy(
            src_ref=weights[c],
            dst_ref=w_recv[c],
            send_sem=ws.at[c],
            recv_sem=wr.at[c],
            device_id=partner,
            device_id_type=MESH,
        )

    def x_copy(d):
        return pltpu.make_async_remote_copy(
            src_ref=x_ref.at[lax.rem(outer + d, lines)],
            dst_ref=x_recv.at[d],
            send_sem=xs.at[d],
            recv_sem=xr.at[d],
            device_id=line_peer(d),
            device_id_type=MESH,
        )

    def p_copy(c, d):
        return pltpu.make_async_remote_copy(
            src_ref=p_send[c].at[d],
            dst_ref=p_recv[c].at[d],
            send_sem=ps.at[c, d],
            recv_sem=pr.at[c, d],
            device_id=line_peer(d),
            device_id_type=MESH,
        )

    for d in range(1, lines):
        x_copy(d).start()
    for c in range(count):
        w_copy(c).start()
    for c in range(count):
        w_copy(c).wait_recv()

        def part(mine, theirs):
            return jnp.dot(mine, weights[c][...], preferred_element_type=f32) + jnp.dot(
                theirs, w_recv[c][...], preferred_element_type=f32
            )

        @pl.loop(1, lines)
        def _(d):
            if c == 0:
                x_copy(d).wait_recv()
            back = lines - d
            p_send[c][back] = part(x_recv[d, inner], x_recv[d, 1 - inner]).astype(bf16)
            p_copy(c, back).start()

        own[c][...] = part(x_ref[outer, inner], x_ref[outer, 1 - inner])
    for c in range(count):

        def add(d, total):
            p_copy(c, d).wait_recv()
            return total + p_recv[c][d].astype(f32)

        outs[c][...] = lax.fori_loop(1, lines, add, own[c][...]).astype(bf16)
    for d in range(1, lines):
        x_copy(d).wait_send()
    for c in range(count):
        w_copy(c).wait_send()

        @pl.loop(1, lines)
        def _(d):
            p_copy(c, d).wait_send()


def project_all(n, x_split, weights):
    lines = n // 2
    rows, depth = x_split.shape[2:]
    count = len(weights)
    widths = [w.shape[1] for w in weights]
    vmem = pl.BlockSpec(memory_space=pltpu.VMEM)
    return pl.pallas_call(
        functools.partial(project_kernel, n, count),
        out_shape=[jax.ShapeDtypeStruct((rows, c), bf16) for c in widths],
        in_specs=[vmem] * (1 + count),
        out_specs=[vmem] * count,
        scratch_shapes=[pltpu.VMEM((lines, 2, rows, depth), bf16)]
        + [pltpu.VMEM((depth, c), bf16) for c in widths]
        + [pltpu.VMEM((lines, rows, c), bf16) for c in widths]
        + [pltpu.VMEM((lines, rows, c), bf16) for c in widths]
        + [pltpu.VMEM((rows, c), f32) for c in widths]
        + [
            pltpu.SemaphoreType.DMA((lines,)),
            pltpu.SemaphoreType.DMA((lines,)),
            pltpu.SemaphoreType.DMA((count,)),
            pltpu.SemaphoreType.DMA((count,)),
            pltpu.SemaphoreType.DMA((count, lines)),
            pltpu.SemaphoreType.DMA((count, lines)),
        ],
        compiler_params=pltpu.CompilerParams(
            collective_id=0, has_side_effects=True, vmem_limit_bytes=VMEM_LIMIT
        ),
    )(x_split, *weights)


def gather_kernel(n, count, *refs):
    ins, outs = refs[:count], refs[count : 2 * count]
    keep, s1, r1, s2, r2 = refs[2 * count :]
    me, lines, outer, inner, partner, line_peer = line_and_pair(n)
    greet([partner] + [line_peer(d) for d in range(1, lines)])

    def along(k, d):
        return pltpu.make_async_remote_copy(
            src_ref=ins[k],
            dst_ref=outs[k].at[me],
            send_sem=s1.at[k, d],
            recv_sem=r1.at[k, d],
            device_id=line_peer(d),
            device_id_type=MESH,
        )

    def across(k, d):
        slot = lax.rem(outer - d + lines, lines) * 2 + inner
        return pltpu.make_async_remote_copy(
            src_ref=ins[k] if isinstance(d, int) and d == 0 else outs[k].at[slot],
            dst_ref=outs[k].at[slot],
            send_sem=s2.at[k, d],
            recv_sem=r2.at[k, d],
            device_id=partner,
            device_id_type=MESH,
        )

    def local(k):
        return pltpu.make_async_copy(ins[k], outs[k].at[me], keep.at[k])

    for k in range(count):

        @pl.loop(1, lines)
        def _(d):
            along(k, d).start()

        across(k, 0).start()
        local(k).start()
    for k in range(count):

        @pl.loop(1, lines)
        def _(d):
            along(k, d).wait_recv()
            across(k, d).start()

    for k in range(count):
        local(k).wait()
        across(k, 0).wait()

        @pl.loop(1, lines)
        def _(d):
            along(k, d).wait_send()
            across(k, d).wait()


def gather_all(n, blocks):
    lines = n // 2
    count = len(blocks)
    vmem = pl.BlockSpec(memory_space=pltpu.VMEM)
    return pl.pallas_call(
        functools.partial(gather_kernel, n, count),
        out_shape=[jax.ShapeDtypeStruct((n,) + b.shape, b.dtype) for b in blocks],
        in_specs=[vmem] * count,
        out_specs=[vmem] * count,
        scratch_shapes=[pltpu.SemaphoreType.DMA((count,))]
        + [pltpu.SemaphoreType.DMA((count, lines))] * 4,
        compiler_params=pltpu.CompilerParams(
            collective_id=1, has_side_effects=True, vmem_limit_bytes=VMEM_LIMIT
        ),
    )(*blocks)


def heads_peer(n, d):
    return {"tp": lax.rem(lax.axis_index("tp") + d, n)}


def latent_kernel(n, in_ref, out_ref, ss, rs, keep):
    me = lax.axis_index("tp")
    greet([heads_peer(n, d) for d in range(1, n)])

    def copy(d):
        return pltpu.make_async_remote_copy(
            src_ref=in_ref,
            dst_ref=out_ref.at[me],
            send_sem=ss.at[d],
            recv_sem=rs.at[d],
            device_id=heads_peer(n, d),
            device_id_type=MESH,
        )

    for d in range(1, n):
        copy(d).start()
    stay = pltpu.make_async_copy(in_ref, out_ref.at[me], keep)
    stay.start()
    stay.wait()
    for d in range(1, n):
        copy(d).wait()


def gather_heads(n, block):
    vmem = pl.BlockSpec(memory_space=pltpu.VMEM)
    return pl.pallas_call(
        functools.partial(latent_kernel, n),
        out_shape=jax.ShapeDtypeStruct((n,) + block.shape, block.dtype),
        in_specs=[vmem],
        out_specs=vmem,
        scratch_shapes=[
            pltpu.SemaphoreType.DMA((n,)),
            pltpu.SemaphoreType.DMA((n,)),
            pltpu.SemaphoreType.DMA,
        ],
        compiler_params=pltpu.CompilerParams(collective_id=2, has_side_effects=True),
    )(block)


def output_kernel(n, mix_ref, w_ref, out_ref, send, recv, ss, rs):
    me = lax.axis_index("tp")
    greet([heads_peer(n, d) for d in range(1, n)])

    def copy(d):
        return pltpu.make_async_remote_copy(
            src_ref=send.at[d],
            dst_ref=recv.at[d],
            send_sem=ss.at[d],
            recv_sem=rs.at[d],
            device_id=heads_peer(n, d),
            device_id_type=MESH,
        )

    for d in range(1, n):
        rows = mix_ref[lax.rem(me + d, n)]
        send[d] = jnp.dot(rows, w_ref[...], preferred_element_type=f32).astype(bf16)
        copy(d).start()
    total = jnp.dot(mix_ref[me], w_ref[...], preferred_element_type=f32)
    for d in range(1, n):
        copy(d).wait_recv()
        total = total + recv[d].astype(f32)
    out_ref[...] = total
    for d in range(1, n):
        copy(d).wait_send()


def output_all(n, mix, weight):
    rows, cols = mix.shape[1], weight.shape[1]
    vmem = pl.BlockSpec(memory_space=pltpu.VMEM)
    return pl.pallas_call(
        functools.partial(output_kernel, n),
        out_shape=jax.ShapeDtypeStruct((rows, cols), f32),
        in_specs=[vmem] * 2,
        out_specs=vmem,
        scratch_shapes=[
            pltpu.VMEM((n, rows, cols), bf16),
            pltpu.VMEM((n, rows, cols), bf16),
            pltpu.SemaphoreType.DMA((n,)),
            pltpu.SemaphoreType.DMA((n,)),
        ],
        compiler_params=pltpu.CompilerParams(
            collective_id=3, has_side_effects=True, vmem_limit_bytes=VMEM_LIMIT
        ),
    )(mix, weight)


def gate_parts(pre_gate, rate_row, seq_len):
    opening = rate_row / seq_len * jax.nn.sigmoid(-pre_gate.astype(f32))
    return (jnp.log1p(-opening), opening)


def on_device(
    tokens,
    input_gain,
    chain_query,
    forward_gate,
    backward_gate,
    chain_value,
    output_gate,
    forget_rate,
    chain_gain,
    query_down,
    latent_down,
    rotary_down,
    query_latent_gain,
    latent_gain,
    query_up,
    latent_up,
    query_head_gain,
    key_head_gain,
    mixer_gain,
    chain_out,
    attend_out,
):
    n_sp, n_tp = lax.axis_size("sp"), lax.axis_size("tp")
    sp, tp = lax.axis_index("sp"), lax.axis_index("tp")
    rows, depth = tokens.shape[0], chain_query.shape[0]
    seq_len = rows * n_sp
    q_cols = query_down.shape[1] // n_tp
    l_cols = latent_down.shape[1] // n_tp
    down = jnp.concatenate(
        [
            lax.dynamic_slice_in_dim(query_down, tp * q_cols, q_cols, 1),
            lax.dynamic_slice_in_dim(latent_down, tp * l_cols, l_cols, 1),
        ],
        axis=1,
    )
    normed = rms_scale(tokens.astype(f32), input_gain).astype(bf16)
    x_split = normed.reshape(rows, n_sp // 2, 2, depth).transpose(1, 2, 0, 3)
    raw, q_rows, fwd_logit, bwd_logit, v_rows, gate_logit = project_all(
        n_sp, x_split, (down, chain_query, forward_gate, backward_gate, chain_value, output_gate)
    )

    def project(source, weight):
        return jnp.dot(source, weight, preferred_element_type=f32).astype(bf16)

    all_raw = gather_heads(n_tp, raw)
    raw_q = all_raw[:, :, :q_cols].transpose(1, 0, 2).reshape(rows, -1).astype(f32)
    raw_l = all_raw[:, :, q_cols:].transpose(1, 0, 2).reshape(rows, -1).astype(f32)
    query_latent = rms_scale(raw_q, query_latent_gain).astype(bf16)
    pair_latent = rms_scale(raw_l, latent_gain).astype(bf16)
    rotary_key = project(normed, rotary_down).astype(f32)
    heads = query_up.shape[1] // ATT_QK
    attend_query = project(query_latent, query_up).astype(f32).reshape(rows, heads, ATT_QK)
    attend_pairs = project(pair_latent, latent_up).reshape(rows, heads, NOPE_DIM + VHEAD_DIM)
    positions = sp * rows + jnp.arange(rows, dtype=jnp.int32)
    query_final = rotate_tail(rms_scale(attend_query, query_head_gain), positions).astype(bf16)
    key_cat = jnp.concatenate(
        [
            attend_pairs[..., :NOPE_DIM].astype(f32),
            jnp.broadcast_to(rotary_key[:, None, :], (rows, heads, ROPE_DIM)),
        ],
        axis=-1,
    )
    key_final = rotate_tail(rms_scale(key_cat, key_head_gain), positions).astype(bf16)
    keys_flat = key_final.reshape(rows, heads * ATT_QK)
    values_flat = attend_pairs[..., NOPE_DIM:].reshape(rows, heads * VHEAD_DIM)

    f_log, f_key = gate_parts(fwd_logit, forget_rate[0], seq_len)
    b_log, b_key = gate_parts(bwd_logit, forget_rate[1], seq_len)
    width = f_log.shape[1]
    chain_heads = width // KEY_DIM
    lower = jnp.tril(jnp.ones((rows, rows), f32))
    f_cum = jnp.dot(lower, f_log, precision=lax.Precision.HIGHEST)
    b_cum = jnp.dot(lower.T, b_log, precision=lax.Precision.HIGHEST)
    q_wide = q_rows.astype(f32)

    def by_head(tensor):
        return tensor.astype(bf16).reshape(rows, chain_heads, -1)

    f_q, f_k = by_head(q_wide * jnp.exp(f_cum)), by_head(f_key * jnp.exp(-f_cum))
    b_q, b_k = by_head(q_wide * jnp.exp(b_cum)), by_head(b_key * jnp.exp(-b_cum))
    v_heads = v_rows.reshape(rows, chain_heads, VAL_DIM)
    logs = jnp.stack([f_cum[-1], b_cum[0]])

    def digest(keys, log):
        state = jnp.einsum("jre,jrw->rew", keys, v_heads, preferred_element_type=f32)
        return state * jnp.exp(log).reshape(chain_heads, KEY_DIM, 1)

    states = jnp.stack([digest(f_k, logs[0]), digest(b_k, logs[1])]).astype(bf16)
    own_out = jnp.concatenate([chain_out, attend_out], axis=0)

    all_keys, all_values, all_states, all_logs, all_out = gather_all(
        n_sp,
        (keys_flat, values_flat, states.reshape(2 * width, VAL_DIM), logs, own_out),
    )

    index = jnp.arange(n_sp)
    before = (index < sp)[:, None]
    after = (index > sp)[:, None]
    between_f = ((index[None, :] > index[:, None]) & (index[None, :] < sp)).astype(f32)
    between_b = ((index[None, :] < index[:, None]) & (index[None, :] > sp)).astype(f32)
    sum_f = jnp.sum(between_f[:, :, None] * all_logs[None, :, 0], axis=1)
    sum_b = jnp.sum(between_b[:, :, None] * all_logs[None, :, 1], axis=1)
    coef = jnp.stack(
        [jnp.where(before, jnp.exp(sum_f), 0.0), jnp.where(after, jnp.exp(sum_b), 0.0)], axis=1
    ).reshape(n_sp, 2 * width, 1)
    entering = jnp.sum(coef * all_states.astype(f32), axis=0).astype(bf16)
    entering = entering.reshape(2, chain_heads, KEY_DIM, VAL_DIM)

    def scores(queries, keys, mask):
        return (
            jnp.einsum("thk,shk->hts", queries, keys, preferred_element_type=f32) * mask
        )

    both = (scores(f_q, f_k, lower) + scores(b_q, b_k, lower.T)).astype(bf16)
    combined = (
        jnp.einsum("hts,shv->thv", both, v_heads, preferred_element_type=f32)
        + jnp.einsum("thk,hkv->thv", f_q, entering[0], preferred_element_type=f32)
        + jnp.einsum("thk,hkv->thv", b_q, entering[1], preferred_element_type=f32)
    )
    head_gain = chain_gain.reshape(chain_heads, VAL_DIM)
    chain_mixed = (
        rms_scale(combined, head_gain).reshape(rows, -1) * jax.nn.silu(gate_logit.astype(f32))
    ).astype(bf16)

    key_all = all_keys.reshape(seq_len, heads, ATT_QK)
    value_all = all_values.reshape(seq_len, heads, VHEAD_DIM)
    weights = jnp.exp(
        jnp.einsum("qhd,khd->hqk", query_final, key_all, preferred_element_type=f32)
        * ATT_QK ** (-0.5)
    )
    numerator = jnp.einsum(
        "hqk,khv->qhv", weights.astype(bf16), value_all, preferred_element_type=f32
    )
    denominator = jnp.sum(weights, axis=-1)
    attend_rows = numerator / jnp.transpose(denominator)[:, :, None]
    attend_mixed = (
        rms_scale(attend_rows, mixer_gain.reshape(heads, VHEAD_DIM))
        .reshape(rows, heads * VHEAD_DIM)
        .astype(bf16)
    )
    mix = jnp.concatenate([chain_mixed, attend_mixed], axis=1)
    full_out = all_out.transpose(1, 0, 2).reshape(mix.shape[1], -1)
    return output_all(n_tp, mix.reshape(n_tp, rows // n_tp, -1), full_out)


def solution(mesh):
    placed = (
        P("sp", None),
        P(),
        P("sp", "tp"),
        P("sp", "tp"),
        P("sp", "tp"),
        P("sp", "tp"),
        P("sp", "tp"),
        P(None, "tp"),
        P("tp"),
        P("sp", None),
        P("sp", None),
        P(),
        P(),
        P(),
        P(None, "tp"),
        P(None, "tp"),
        P(),
        P(),
        P("tp"),
        P("tp", "sp"),
        P("tp", "sp"),
    )
    return jax.shard_map(
        on_device, mesh=mesh, in_specs=placed, out_specs=P(("sp", "tp"), None), check_vma=False
    )
```

time: 430 us -> 197 us (0.46)
  waiting for transfers between devices: 195 us -> 0 us
  blocking collectives: 165 us -> 0 us
  Pallas kernels: 0 us -> 161 us
  matrix products: 22.4 us -> 6.34 us
  between operations: 14.3 us -> 0.62 us
  other arithmetic: 21.7 us -> 14.3 us
  local copies, waits for them, and re-layouts: 9.24 us -> 13.9 us
    all_gather x8 -> x0, blocking collectives: 165 us -> none  [the longest x2 29.2 us: entering(): everything = jax.tree.map(lambda part: lax.all_gather(part, axis), value)]
    all_gather x9 -> x0, waiting for transfers between devices: 162 us -> none  [the longest x1 38.7 us: on_device(): lax.all_gather(backward_gate, 'sp', axis=0, tiled=True)]
    pallas_call x0 -> x4, Pallas kernels: none -> 161 us  [the longest x1 69.2 us: gather_all(): pl.pallas_call(functools.partial(gather_kernel, n, count), out_shape=[jax...]
    reduce_scatter x1 -> x0, waiting for transfers between devices: 27.9 us -> none  [on_device(): lax.psum_scatter(row_term(chain_mixed, full_chain_out) + row_term(attend_...]
    dot_general x21 -> x13, matrix products: 22.4 us -> 6.34 us  [the longest x3 1.96 us: project(): return jnp.dot(source, weight, preferred_element_type=f32).astype(bf16)]
    select_n x17 -> x4, other arithmetic: 16.6 us -> 0.85 us  [the longest x2 0.71 us: on_device(): lower = jnp.tril(jnp.ones((rows, rows), f32))]
    reshape x4 -> x7, local copies, waits for them, and re-layouts: 0.31 us -> 5.14 us  [the longest x1 1.62 us: on_device(): full_out = all_out.transpose(1, 0, 2).reshape(mix.shape[1], -1)]
    unnamed x10 -> x0, waiting for transfers between devices: 4.73 us -> none
  transfers between devices with their start and end apart: 10 -> 0, of which waited for: 6 -> 0; matrix products, arithmetic and copies ran while one was open for 12% -> 0% of each run, Pallas kernels for 0% -> 0%
where the time goes in v1:
time: 197 us; the launch traced here: 196 us
  Pallas kernels  161 us (82%)
  other arithmetic  14.3 us (7%)
  local copies, waits for them, and re-layouts  13.9 us (7%)
  matrix products  6.34 us (3%)
    pallas_call x1, Pallas kernels, gather_all(): pl.pallas_call(functools.partial(gather_kernel, n, count), out_shape=[jax...  69.2 us
    pallas_call x1, Pallas kernels, project_all(): pl.pallas_call(functools.partial(project_kernel, n, count), out_shape=[ja...  63.1 us
    pallas_call x1, Pallas kernels, gather_heads(): pl.pallas_call(functools.partial(latent_kernel, n), out_shape=jax.ShapeDt...  15.1 us
    pallas_call x1, Pallas kernels, output_all(): pl.pallas_call(functools.partial(output_kernel, n), out_shape=jax.ShapeDt...  13.5 us
    reduce_sum x5, other arithmetic, rms_scale(): mean_square = jnp.mean(values * values, axis=-1, keepdims=True)  4.19 us

profile of v1, /device:TPU:1, one launch (start us, length us, event | category | flops | bytes accessed | tf_op | source)
XLA Modules:
  0.0 196.1 jit_solution(3055075774211041601)
XLA Ops:
  0.1 1.4 fusion.1
  1.5 0.8 slice_multiply_fusion.1
  2.3 0.9 constant_dynamic-slice_fusion
  3.1 1.0 constant_dynamic-slice_fusion.1
  4.2 0.8 pad_maximum_fusion.2.refs_0_
  5.3 0.7 fusion.54
  6.1 0.7 pad_maximum_fusion.1.refs_4_
  7.8 1.0 copy.219
  8.8 63.1 %shard_map.199 = (bf16[160,320]{1,0:T(8,128)(2,1)}, bf16[160,256]{1,0:T(8,128)(2,1)}, bf16[160,256]{1,0:T(8,128)(2,1)}, bf16[160,256]{1,0:T(8,128)(2,1)}, bf16[1...) custom-call(bf16[4,2,160,256]{3,2,1,0:T(8,128)(2,1)} %bitcast.129, bf16[256,320]{1,0:T(8,128)(2,1)} %pad_maximum_fusion.2.refs_0_, ...), custom_call_target="tpu_custom_call" | custom-call | tf_op jit(solution)/shard_map/pallas_call | solution.py:155
  72.1 1.3 fusion.49
  74.0 0.6 pad_maximum_fusion.7.refs_3_
  75.1 0.7 pad_maximum_fusion.5
  76.0 15.1 %shard_map.200 = bf16[4,160,320]{2,1,0:T(8,128)(2,1)} custom-call(bf16[160,320]{1,0:T(8,128)(2,1)} %get-tuple-element.20.in_ref), custom_call_target="tpu_custom_call" | custom-call | tf_op jit(solution)/shard_map/pallas_call | solution.py:280
  91.1 1.2 fusion.21
  92.3 1.2 fusion.19
  93.6 1.3 convolution_convert_fusion
  95.0 0.6 copy.220
  98.0 0.8 subtract_convert_fusion
  98.8 0.6 slice.106
  99.7 0.8 convert_element_type.162.refs_0_
  100.5 69.2 %shard_map.201 = (bf16[8,160,384]{2,1,0:T(8,128)(2,1)}, bf16[8,160,256]{2,1,0:T(8,128)(2,1)}, bf16[8,512,128]{2,1,0:T(8,128)(2,1)}, f32[8,2,256]{2,1,0:T(2,128)}, bf16[8,512,256]{2,1,0:T(8,128)(2,1)}) custom-call(bf16[160,384]{1,0:T(8,128)(2,1)} %convert_element_type.162.refs_0_, bf16[160,256]{1,0:T(8,128)(2,1)} %bitcast.133, bf16[512,128]{1,0:T(8,128)(2,1)} %bitcast.132, ...), custom_call_target="tpu_custom_call" | custom-call | tf_op jit(solution)/shard_map/pallas_call | solution.py:238
  169.7 0.8 fusion.107
  170.8 1.8 multiply_reduce_fusion
  173.5 1.0 fusion.52
  174.5 1.0 reshape.360
  175.5 0.8 reshape.363
  176.5 0.7 fusion.108
  177.6 0.5 multiply_reduce_fusion.2
  178.2 0.7 pad_maximum_fusion.4
  179.2 1.6 copy.143
  180.8 13.5 %shard_map.202 = f32[40,2048]{1,0:T(8,128)} custom-call(bf16[4,40,512]{2,1,0:T(8,128)(2,1)} %bitcast.131, bf16[512,2048]{1,0:T(8,128)(2,1)} %bitcast.128), custom_call_target="tpu_custom_call" | custom-call | tf_op jit(solution)/shard_map/pallas_call | solution.py:324
  194.4 1.7 copy.224
  (104 shorter events, 7.6 us)
Async XLA Ops:
  0.0 96.8 %copy-start = (bf16[768,384]{1,0:T(8,128)(2,1)S(1)}, bf16[768,384]{1,0:T(8,128)(2,1)}, u32[]{:S(2)}) copy-start(bf16[768,384]{1,0:T(8,128)(2,1)} %param.35) | copy-start | bytes 1769476
  0.0 6.8 %copy-start.2 = (bf16[160,2048]{1,0:T(8,128)(2,1)S(1)}, bf16[160,2048]{1,0:T(8,128)(2,1)}, u32[]{:S(2)}) copy-start(bf16[160,2048]{1,0:T(8,128)(2,1)} %param.21) | copy-start | bytes 1966084
  0.0 6.0 %copy-start.9 = (bf16[256,256]{1,0:T(8,128)(2,1)S(1)}, bf16[256,256]{1,0:T(8,128)(2,1)}, u32[]{:S(2)}) copy-start(bf16[256,256]{1,0:T(8,128)(2,1)} %param.41) | copy-start | bytes 393220
  0.0 6.0 %copy-start.10 = (bf16[256,256]{1,0:T(8,128)(2,1)S(1)}, bf16[256,256]{1,0:T(8,128)(2,1)}, u32[]{:S(2)}) copy-start(bf16[256,256]{1,0:T(8,128)(2,1)} %param.40) | copy-start | bytes 393220
  0.0 6.8 %copy-start.18 = (f32[2048]{0:T(1024)S(1)}, f32[2048]{0:T(1024)}, u32[]{:S(2)}) copy-start(f32[2048]{0:T(1024)} %param.22) | copy-start | bytes 24580
  4.2 2.8 %copy-start.8 = (bf16[2048,64]{0,1:T(8,128)(2,1)S(1)}, bf16[2048,64]{0,1:T(8,128)(2,1)}, u32[]{:S(2)}) copy-start(bf16[2048,64]{0,1:T(8,128)(2,1)} %param.32) | copy-start | bytes 786436
  71.9 1.5 copy-start.16
  71.9 1.9 copy-start.14
  71.9 1.9 copy-start.15
  72.0 2.6 %copy-start.11 = (bf16[160,256]{1,0:T(8,128)(2,1)S(1)}, bf16[160,256]{1,0:T(8,128)(2,1)}, u32[]{:S(2)}) copy-start(bf16[160,256]{1,0:T(8,128)(2,1)} %get-tuple-element.16) | copy-start | bytes 245764
  74.0 19.5 %copy-start.24 = (bf16[512,512]{1,0:T(8,128)(2,1)S(1)}, bf16[512,512]{1,0:T(8,128)(2,1)}, u32[]{:S(2)}) copy-start(bf16[512,512]{1,0:T(8,128)(2,1)} %param.36) | copy-start | bytes 1572868
  74.0 19.5 %copy-start.25 = (f32[512]{0:T(512)S(1)}, f32[512]{0:T(512)}, u32[]{:S(2)}) copy-start(f32[512]{0:T(512)} %param.34) | copy-start | bytes 6148
  92.3 3.5 %copy-start.1 = (bf16[4,160,320]{2,1,0:T(8,128)(2,1)S(1)}, bf16[4,160,320]{2,1,0:T(8,128)(2,1)}, u32[]{:S(2)}) copy-start(bf16[4,160,320]{2,1,0:T(8,128)(2,1)} %shard_map.200) | copy-start | bytes 1228804
  95.9 0.9 copy-start.19
  96.8 1.0 copy-start.20
  96.8 1.0 copy-start.21
  100.5 72.5 %copy-start.5 = (f32[160,160]{1,0:T(8,128)S(1)}, f32[160,160]{1,0:T(8,128)}, u32[]{:S(2)}) copy-start(f32[160,160]{1,0:T(8,128)} %fusion.54) | copy-start | bytes 307204
  172.6 0.9 copy-start.22
  172.6 1.9 copy-start.6
  173.0 2.5 %copy-start.4 = (bf16[8,160,384]{2,1,0:T(8,128)(2,1)S(1)}, bf16[8,160,384]{2,1,0:T(8,128)(2,1)}, u32[]{:S(2)}) copy-start(bf16[8,160,384]{2,1,0:T(8,128)(2,1)} %get-tuple-element.25) | copy-start | bytes 2949124
  175.5 0.9 copy-start.12
  175.5 0.9 copy-start.13
  175.5 1.0 copy-start.17
  176.5 1.1 copy-start.7
  177.2 0.9 copy-start.23
  177.6 1.6 copy-start.3

commit v2 on v1

v2 whole, which is shorter than its diff:
```python
import functools

import jax
import jax.numpy as jnp
from jax import lax
from jax.experimental import pallas as pl
from jax.experimental.pallas import tpu as pltpu
from jax.sharding import PartitionSpec as P

KEY_DIM = 128
VAL_DIM = 128
NOPE_DIM = 128
ROPE_DIM = 64
VHEAD_DIM = 128
ATT_QK = 192

norm_eps = 1e-06
rope_theta = 10000.0
MESH = pl.DeviceIdType.MESH
VMEM_LIMIT = 60 * 1024 * 1024
f32 = jnp.float32
bf16 = jnp.bfloat16


def rms_scale(values, gain_vec):
    mean_square = jnp.mean(values * values, axis=-1, keepdims=True)
    return values * lax.rsqrt(mean_square + norm_eps) * gain_vec


def rotate_tail(values, positions):
    half_dim = ROPE_DIM // 2
    inverse = rope_theta ** (-jnp.arange(0, ROPE_DIM, 2).astype(f32) / ROPE_DIM)
    angles = positions.astype(f32)[:, None] * inverse
    cosine = jnp.cos(angles)[:, None, :]
    sine_table = jnp.sin(angles)[:, None, :]
    unrotated = values[..., :NOPE_DIM]
    first_half = values[..., NOPE_DIM : NOPE_DIM + half_dim]
    latter = values[..., NOPE_DIM + half_dim :]
    return jnp.concatenate(
        [
            unrotated,
            first_half * cosine - latter * sine_table,
            latter * cosine + first_half * sine_table,
        ],
        axis=-1,
    )


def greet(peers):
    barrier = pltpu.get_barrier_semaphore()
    for peer in peers:
        pl.semaphore_signal(barrier, inc=1, device_id=peer, device_id_type=MESH)
    pl.semaphore_wait(barrier, len(peers))


def line_and_pair(n):
    me = lax.axis_index("sp")
    lines = n // 2
    outer, inner = me // 2, lax.rem(me, 2)
    partner = {"sp": outer * 2 + 1 - inner}

    def line_peer(d):
        return {"sp": lax.rem(outer + d, lines) * 2 + inner}

    return me, lines, outer, inner, partner, line_peer


def project_kernel(n, count, x_ref, *refs):
    weights = refs[:count]
    outs = refs[count : 2 * count]
    rest = refs[2 * count :]
    x_recv = rest[0]
    w_recv = rest[1 : 1 + count]
    p_send = rest[1 + count : 1 + 2 * count]
    p_recv = rest[1 + 2 * count : 1 + 3 * count]
    own = rest[1 + 3 * count : 1 + 4 * count]
    xs, xr, ws, wr, ps, pr = rest[1 + 4 * count :]
    groups = n // 4
    me = lax.axis_index("sp")
    group, place = me // 4, lax.rem(me, 4)
    low, inner = place // 2, lax.rem(place, 2)
    places = (
        place,
        (1 - low) * 2 + inner,
        low * 2 + 1 - inner,
        (1 - low) * 2 + 1 - inner,
    )
    beside = {"sp": group * 4 + places[1]}
    partner = {"sp": group * 4 + places[2]}

    def far_peer(d):
        return {"sp": lax.rem(group + d, groups) * 4 + place}

    greet([beside, partner] + [far_peer(d) for d in range(1, groups)])

    def w_copy(c, k):
        return pltpu.make_async_remote_copy(
            src_ref=w_recv[c].at[0] if k == 2 else weights[c],
            dst_ref=w_recv[c].at[k],
            send_sem=ws.at[c, k],
            recv_sem=wr.at[c, k],
            device_id=beside if k == 0 else partner,
            device_id_type=MESH,
        )

    def x_copy(d):
        return pltpu.make_async_remote_copy(
            src_ref=x_ref.at[lax.rem(group + d, groups)],
            dst_ref=x_recv.at[d],
            send_sem=xs.at[d],
            recv_sem=xr.at[d],
            device_id=far_peer(d),
            device_id_type=MESH,
        )

    def p_copy(c, d):
        return pltpu.make_async_remote_copy(
            src_ref=p_send[c].at[d],
            dst_ref=p_recv[c].at[d],
            send_sem=ps.at[c, d],
            recv_sem=pr.at[c, d],
            device_id=far_peer(d),
            device_id_type=MESH,
        )

    w_copy(0, 0).start()
    w_copy(0, 1).start()
    for d in range(1, groups):
        x_copy(d).start()
    for c in range(1, count):
        w_copy(c, 0).start()
    for c in range(count):
        w_copy(c, 0).wait_recv()
        w_copy(c, 2).start()
        if c + 1 < count:
            w_copy(c + 1, 1).start()
    for c in range(count):
        w_copy(c, 1).wait_recv()
        w_copy(c, 2).wait_recv()

        def part(x):
            total = jnp.dot(x(places[0]), weights[c][...], preferred_element_type=f32)
            for k in range(3):
                total += jnp.dot(x(places[k + 1]), w_recv[c][k], preferred_element_type=f32)
            return total

        @pl.loop(1, groups)
        def _(d):
            if c == 0:
                x_copy(d).wait_recv()
            back = groups - d
            p_send[c][back] = part(lambda k: x_recv[d, k]).astype(bf16)
            p_copy(c, back).start()

        own[c][...] = part(lambda k: x_ref[group, k])
    for c in range(count):

        def add(d, total):
            p_copy(c, d).wait_recv()
            return total + p_recv[c][d].astype(f32)

        outs[c][...] = lax.fori_loop(1, groups, add, own[c][...]).astype(bf16)
    for d in range(1, groups):
        x_copy(d).wait_send()
    for c in range(count):
        for k in range(3):
            w_copy(c, k).wait_send()

        @pl.loop(1, groups)
        def _(d):
            p_copy(c, d).wait_send()


def project_all(n, x_split, weights):
    groups = n // 4
    rows, depth = x_split.shape[2:]
    count = len(weights)
    widths = [w.shape[1] for w in weights]
    vmem = pl.BlockSpec(memory_space=pltpu.VMEM)
    return pl.pallas_call(
        functools.partial(project_kernel, n, count),
        out_shape=[jax.ShapeDtypeStruct((rows, c), bf16) for c in widths],
        in_specs=[vmem] * (1 + count),
        out_specs=[vmem] * count,
        scratch_shapes=[pltpu.VMEM((groups, 4, rows, depth), bf16)]
        + [pltpu.VMEM((3, depth, c), bf16) for c in widths]
        + [pltpu.VMEM((groups, rows, c), bf16) for c in widths]
        + [pltpu.VMEM((groups, rows, c), bf16) for c in widths]
        + [pltpu.VMEM((rows, c), f32) for c in widths]
        + [
            pltpu.SemaphoreType.DMA((groups,)),
            pltpu.SemaphoreType.DMA((groups,)),
            pltpu.SemaphoreType.DMA((count, 3)),
            pltpu.SemaphoreType.DMA((count, 3)),
            pltpu.SemaphoreType.DMA((count, groups)),
            pltpu.SemaphoreType.DMA((count, groups)),
        ],
        compiler_params=pltpu.CompilerParams(
            collective_id=0, has_side_effects=True, vmem_limit_bytes=VMEM_LIMIT
        ),
    )(x_split, *weights)


def gather_kernel(n, heads_n, *refs):
    count = 5
    query_in, pair_in, ins = refs[0], refs[1], refs[2 : 2 + count]
    query_out, pair_out, outs = refs[2 + count], refs[3 + count], refs[4 + count : 4 + 2 * count]
    keep, s1, r1, s2, r2, hs1, hr1, hs2, hr2 = refs[4 + 2 * count :]
    me, lines, outer, inner, partner, line_peer = line_and_pair(n)
    head = lax.axis_index("tp")
    head_lines = heads_n // 2
    head_outer, head_inner = head // 2, lax.rem(head, 2)
    head_partner = {"tp": head_outer * 2 + 1 - head_inner}

    def head_peer(d):
        return {"tp": lax.rem(head_outer + d, head_lines) * 2 + head_inner}

    greet(
        [partner, head_partner]
        + [line_peer(d) for d in range(1, lines)]
        + [head_peer(d) for d in range(1, head_lines)]
    )
    src = (pair_in,) + tuple(ins)

    def slot(k, at):
        return pair_out.at[head, at] if k == 0 else outs[k - 1].at[at]

    def along(k, d):
        return pltpu.make_async_remote_copy(
            src_ref=src[k],
            dst_ref=slot(k, me),
            send_sem=s1.at[k, d],
            recv_sem=r1.at[k, d],
            device_id=line_peer(d),
            device_id_type=MESH,
        )

    def across(k, d):
        at = lax.rem(outer - d + lines, lines) * 2 + inner
        return pltpu.make_async_remote_copy(
            src_ref=src[k] if isinstance(d, int) and d == 0 else slot(k, at),
            dst_ref=slot(k, at),
            send_sem=s2.at[k, d],
            recv_sem=r2.at[k, d],
            device_id=partner,
            device_id_type=MESH,
        )

    def local(k):
        return pltpu.make_async_copy(src[k], slot(k, me), keep.at[k])

    def head_along(j, d):
        return pltpu.make_async_remote_copy(
            src_ref=query_in if j == 0 else pair_out.at[head],
            dst_ref=query_out.at[head] if j == 0 else pair_out.at[head],
            send_sem=hs1.at[j, d],
            recv_sem=hr1.at[j, d],
            device_id=head_peer(d),
            device_id_type=MESH,
        )

    def head_across(j, d):
        at = lax.rem(head_outer - d + head_lines, head_lines) * 2 + head_inner
        own = isinstance(d, int) and d == 0
        out = query_out if j == 0 else pair_out
        return pltpu.make_async_remote_copy(
            src_ref=query_in if j == 0 and own else out.at[at],
            dst_ref=out.at[at],
            send_sem=hs2.at[j, d],
            recv_sem=hr2.at[j, d],
            device_id=head_partner,
            device_id_type=MESH,
        )

    query_local = pltpu.make_async_copy(query_in, query_out.at[head], keep.at[1 + count])

    def needed(k, there):
        if k == 2:
            return there
        if k == 3:
            return jnp.logical_not(there)
        return None

    def maybe(condition, act):
        if condition is None:
            act()
        else:
            pl.when(condition)(act)

    def on_line(k, sending, act):
        @pl.loop(1, lines)
        def _(d):
            there = outer + d < lines if sending else outer >= d
            maybe(needed(k, there), lambda: act(d))

    for k in range(1 + count):
        on_line(k, True, lambda d: along(k, d).start())
        across(k, 0).start()
        local(k).start()
        if k == 0:
            for d in range(1, head_lines):
                head_along(0, d).start()
            head_across(0, 0).start()
            query_local.start()

    def pass_on(k):
        def act(d):
            along(k, d).wait_recv()
            across(k, d).start()

        on_line(k, False, act)

    pass_on(0)
    for d in range(1, head_lines):
        head_along(0, d).wait_recv()
        head_across(0, d).start()
    local(0).wait()
    across(0, 0).wait_recv()
    on_line(0, False, lambda d: across(0, d).wait_recv())
    for d in range(1, head_lines):
        head_along(1, d).start()
    head_across(1, 0).start()
    for k in range(1, count - 1):
        pass_on(k)
    for d in range(1, head_lines):
        head_along(1, d).wait_recv()
        head_across(1, d).start()
    for k in range(count - 1, 1 + count):
        pass_on(k)

    query_local.wait()
    for k in range(1 + count):
        across(k, 0).wait_send()
        if k > 0:
            local(k).wait()
            across(k, 0).wait_recv()
        on_line(k, True, lambda d: along(k, d).wait_send())

        def act(d):
            across(k, d).wait_send()
            if k > 0:
                across(k, d).wait_recv()

        on_line(k, False, act)
    for j in range(2):
        head_across(j, 0).wait()
        for d in range(1, head_lines):
            head_along(j, d).wait_send()
            head_across(j, d).wait()


def gather_all(n, heads_n, query, pair, blocks):
    lines, head_lines = n // 2, heads_n // 2
    count = len(blocks)
    vmem = pl.BlockSpec(memory_space=pltpu.VMEM)
    return pl.pallas_call(
        functools.partial(gather_kernel, n, heads_n),
        out_shape=[
            jax.ShapeDtypeStruct((heads_n,) + query.shape, query.dtype),
            jax.ShapeDtypeStruct((heads_n, n) + pair.shape, pair.dtype),
        ]
        + [jax.ShapeDtypeStruct((n,) + b.shape, b.dtype) for b in blocks],
        in_specs=[vmem] * (2 + count),
        out_specs=[vmem] * (2 + count),
        scratch_shapes=[pltpu.SemaphoreType.DMA((2 + count,))]
        + [pltpu.SemaphoreType.DMA((1 + count, lines))] * 4
        + [pltpu.SemaphoreType.DMA((2, head_lines))] * 4,
        compiler_params=pltpu.CompilerParams(
            collective_id=1, has_side_effects=True, vmem_limit_bytes=VMEM_LIMIT
        ),
    )(query, pair, *blocks)


def heads_peer(n, d):
    return {"tp": lax.rem(lax.axis_index("tp") + d, n)}


def output_kernel(n, chain_ref, attend_ref, wc_ref, wa_ref, out_ref, send, recv, ss, rs):
    me = lax.axis_index("tp")
    greet([heads_peer(n, d) for d in range(1, n)])

    def copy(d):
        return pltpu.make_async_remote_copy(
            src_ref=send.at[d],
            dst_ref=recv.at[d],
            send_sem=ss.at[d],
            recv_sem=rs.at[d],
            device_id=heads_peer(n, d),
            device_id_type=MESH,
        )

    def rows_of(at):
        chain, attend = chain_ref[at], attend_ref[at]
        return jnp.concatenate(
            [
                jnp.dot(chain, wc_ref[s], preferred_element_type=f32)
                + jnp.dot(attend, wa_ref[s], preferred_element_type=f32)
                for s in range(wc_ref.shape[0])
            ],
            axis=1,
        )

    for d in range(1, n):
        send[d] = rows_of(lax.rem(me + d, n)).astype(bf16)
        copy(d).start()
    total = rows_of(me)
    for d in range(1, n):
        copy(d).wait_recv()
        total = total + recv[d].astype(f32)
    out_ref[...] = total
    for d in range(1, n):
        copy(d).wait_send()


def output_all(n, chain, attend, chain_w, attend_w):
    rows, cols = chain.shape[1], chain_w.shape[0] * chain_w.shape[2]
    vmem = pl.BlockSpec(memory_space=pltpu.VMEM)
    return pl.pallas_call(
        functools.partial(output_kernel, n),
        out_shape=jax.ShapeDtypeStruct((rows, cols), f32),
        in_specs=[vmem] * 4,
        out_specs=vmem,
        scratch_shapes=[
            pltpu.VMEM((n, rows, cols), bf16),
            pltpu.VMEM((n, rows, cols), bf16),
            pltpu.SemaphoreType.DMA((n,)),
            pltpu.SemaphoreType.DMA((n,)),
        ],
        compiler_params=pltpu.CompilerParams(
            collective_id=3, has_side_effects=True, vmem_limit_bytes=VMEM_LIMIT
        ),
    )(chain, attend, chain_w, attend_w)


def gate_parts(pre_gate, rate_row, seq_len):
    opening = rate_row / seq_len * jax.nn.sigmoid(-pre_gate.astype(f32))
    return (jnp.log1p(-opening), opening)


def on_device(
    tokens,
    input_gain,
    chain_query,
    forward_gate,
    backward_gate,
    chain_value,
    output_gate,
    forget_rate,
    chain_gain,
    query_down,
    latent_down,
    rotary_down,
    query_latent_gain,
    latent_gain,
    query_up,
    latent_up,
    query_head_gain,
    key_head_gain,
    mixer_gain,
    chain_out,
    attend_out,
):
    n_sp, n_tp = lax.axis_size("sp"), lax.axis_size("tp")
    sp, tp = lax.axis_index("sp"), lax.axis_index("tp")
    rows, depth = tokens.shape[0], chain_query.shape[0]
    seq_len = rows * n_sp
    q_cols = query_down.shape[1] // n_tp
    l_cols = latent_down.shape[1] // n_tp
    r_cols = ROPE_DIM // n_tp
    q_down = lax.dynamic_slice_in_dim(query_down, tp * q_cols, q_cols, 1)
    l_down = jnp.concatenate(
        [
            lax.dynamic_slice_in_dim(latent_down, tp * l_cols, l_cols, 1),
            lax.dynamic_slice(rotary_down, (sp * depth, tp * r_cols), (depth, r_cols)),
        ],
        axis=1,
    )
    normed = rms_scale(tokens.astype(f32), input_gain).astype(bf16)
    x_split = normed.reshape(rows, n_sp // 4, 4, depth).transpose(1, 2, 0, 3)
    raw_q, raw_l, q_rows, fwd_logit, bwd_logit, v_rows, gate_logit = project_all(
        n_sp,
        x_split,
        (q_down, l_down, chain_query, forward_gate, backward_gate, chain_value, output_gate),
    )

    def project(source, weight):
        return jnp.dot(source, weight, preferred_element_type=f32).astype(bf16)

    f_log, f_key = gate_parts(fwd_logit, forget_rate[0], seq_len)
    b_log, b_key = gate_parts(bwd_logit, forget_rate[1], seq_len)
    width = f_log.shape[1]
    chain_heads = width // KEY_DIM
    lower = jnp.tril(jnp.ones((rows, rows), f32))
    f_cum = jnp.dot(lower, f_log, precision=lax.Precision.HIGHEST)
    b_cum = jnp.dot(lower.T, b_log, precision=lax.Precision.HIGHEST)
    q_wide = q_rows.astype(f32)

    def by_head(tensor):
        return tensor.astype(bf16).reshape(rows, chain_heads, -1)

    f_q, f_k = by_head(q_wide * jnp.exp(f_cum)), by_head(f_key * jnp.exp(-f_cum))
    b_q, b_k = by_head(q_wide * jnp.exp(b_cum)), by_head(b_key * jnp.exp(-b_cum))
    v_heads = v_rows.reshape(rows, chain_heads, VAL_DIM)
    logs = jnp.stack([f_cum[-1], b_cum[0]])

    def digest(keys, log):
        state = jnp.einsum("jre,jrw->rew", keys, v_heads, preferred_element_type=f32)
        return state * jnp.exp(log).reshape(chain_heads, KEY_DIM, 1)

    f_state, b_state = digest(f_k, logs[0]).astype(bf16), digest(b_k, logs[1]).astype(bf16)

    query_raw, pair_raw, all_logs, all_f, all_b, all_chain, all_attend = gather_all(
        n_sp,
        n_tp,
        raw_q,
        raw_l,
        (
            logs,
            f_state.reshape(width, VAL_DIM),
            b_state.reshape(width, VAL_DIM),
            chain_out,
            attend_out,
        ),
    )

    index = jnp.arange(n_sp)
    before = (index < sp)[:, None]
    after = (index > sp)[:, None]
    between_f = ((index[None, :] > index[:, None]) & (index[None, :] < sp)).astype(f32)
    between_b = ((index[None, :] < index[:, None]) & (index[None, :] > sp)).astype(f32)
    sum_f = jnp.sum(between_f[:, :, None] * all_logs[None, :, 0], axis=1)
    sum_b = jnp.sum(between_b[:, :, None] * all_logs[None, :, 1], axis=1)
    def entering(mask, log_sum, states):
        wide = jnp.exp(log_sum)[:, :, None] * states.astype(f32)
        total = jnp.sum(jnp.where(mask[:, :, None], wide, 0.0), axis=0)
        return total.astype(bf16).reshape(chain_heads, KEY_DIM, VAL_DIM)

    f_in, b_in = entering(before, sum_f, all_f), entering(after, sum_b, all_b)

    def scores(queries, keys, mask):
        return (
            jnp.einsum("thk,shk->hts", queries, keys, preferred_element_type=f32) * mask
        )

    both = (scores(f_q, f_k, lower) + scores(b_q, b_k, lower.T)).astype(bf16)
    combined = (
        jnp.einsum("hts,shv->thv", both, v_heads, preferred_element_type=f32)
        + jnp.einsum("thk,hkv->thv", f_q, f_in, preferred_element_type=f32)
        + jnp.einsum("thk,hkv->thv", b_q, b_in, preferred_element_type=f32)
    )
    head_gain = chain_gain.reshape(chain_heads, VAL_DIM)
    chain_mixed = (
        rms_scale(combined, head_gain).reshape(rows, -1) * jax.nn.silu(gate_logit.astype(f32))
    ).astype(bf16)

    heads = query_up.shape[1] // ATT_QK
    query_latent = rms_scale(
        query_raw.transpose(1, 0, 2).reshape(rows, -1).astype(f32), query_latent_gain
    ).astype(bf16)
    pair_rows = pair_raw.transpose(1, 2, 0, 3)
    pair_latent = rms_scale(
        pair_rows[..., :l_cols].reshape(seq_len, -1).astype(f32), latent_gain
    ).astype(bf16)
    rotary_key = pair_rows[..., l_cols:].reshape(seq_len, ROPE_DIM).astype(f32)
    attend_query = project(query_latent, query_up).astype(f32).reshape(rows, heads, ATT_QK)
    attend_pairs = project(pair_latent, latent_up).reshape(seq_len, heads, NOPE_DIM + VHEAD_DIM)
    query_final = rotate_tail(
        rms_scale(attend_query, query_head_gain), sp * rows + jnp.arange(rows, dtype=jnp.int32)
    ).astype(bf16)
    key_cat = jnp.concatenate(
        [
            attend_pairs[..., :NOPE_DIM].astype(f32),
            jnp.broadcast_to(rotary_key[:, None, :], (seq_len, heads, ROPE_DIM)),
        ],
        axis=-1,
    )
    key_all = rotate_tail(
        rms_scale(key_cat, key_head_gain), jnp.arange(seq_len, dtype=jnp.int32)
    ).astype(bf16)
    value_all = attend_pairs[..., NOPE_DIM:]
    weights = jnp.exp(
        jnp.einsum("qhd,khd->hqk", query_final, key_all, preferred_element_type=f32)
        * ATT_QK ** (-0.5)
    )
    numerator = jnp.einsum(
        "hqk,khv->qhv", weights.astype(bf16), value_all, preferred_element_type=f32
    )
    denominator = jnp.sum(weights, axis=-1)
    attend_rows = numerator / jnp.transpose(denominator)[:, :, None]
    attend_mixed = (
        rms_scale(attend_rows, mixer_gain.reshape(heads, VHEAD_DIM))
        .reshape(rows, heads * VHEAD_DIM)
        .astype(bf16)
    )
    def row_blocks(tensor):
        return tensor.reshape(n_tp, rows // n_tp, -1)

    return output_all(
        n_tp, row_blocks(chain_mixed), row_blocks(attend_mixed), all_chain, all_attend
    )


def solution(mesh):
    placed = (
        P("sp", None),
        P(),
        P("sp", "tp"),
        P("sp", "tp"),
        P("sp", "tp"),
        P("sp", "tp"),
        P("sp", "tp"),
        P(None, "tp"),
        P("tp"),
        P("sp", None),
        P("sp", None),
        P(),
        P(),
        P(),
        P(None, "tp"),
        P(None, "tp"),
        P(),
        P(),
        P("tp"),
        P("tp", "sp"),
        P("tp", "sp"),
    )
    return jax.shard_map(
        on_device, mesh=mesh, in_specs=placed, out_specs=P(("sp", "tp"), None), check_vma=False
    )
```

time: 197 us -> 172 us (0.87)
  Pallas kernels: 161 us -> 129 us
  other arithmetic: 14.3 us -> 17.6 us
  local copies, waits for them, and re-layouts: 13.9 us -> 16.3 us
    pallas_call x2 -> x1, Pallas kernels: 84.3 us -> 51.9 us  [gather_all(): pl.pallas_call(functools.partial(gather_kernel, n, heads_n), out_shape=[j...]
    convert_element_type x4 -> x7, local copies, waits for them, and re-layouts: 1.72 us -> 6.46 us  [the longest x2 3.19 us: on_device(): rotary_key = pair_rows[..., l_cols:].reshape(seq_len, ROPE_DIM).astype(f32)]
    reshape x6 -> x2, local copies, waits for them, and re-layouts: 4.9 us -> 1.43 us  [on_device(): x_split = normed.reshape(rows, n_sp // 4, 4, depth).transpose(1, 2, 0, 3)]
    convert_element_type x1 -> x3, other arithmetic: 0.05 us -> 3.27 us  [the longest x1 1.62 us: on_device(): pair_rows[..., :l_cols].reshape(seq_len, -1).astype(f32)]
    pallas_call x1, Pallas kernels: 13.5 us -> 15.6 us  [output_all(): pl.pallas_call(functools.partial(output_kernel, n), out_shape=jax.ShapeDt...]
where the time goes in v2:
time: 172 us; the launch traced here: 171 us
  Pallas kernels  129 us (75%)
  other arithmetic  17.6 us (10%)
  local copies, waits for them, and re-layouts  16.3 us (9%)
  matrix products  7.78 us (5%)
    pallas_call x1, Pallas kernels, project_all(): pl.pallas_call(functools.partial(project_kernel, n, count), out_shape=[ja...  61.5 us
    pallas_call x1, Pallas kernels, gather_all(): pl.pallas_call(functools.partial(gather_kernel, n, heads_n), out_shape=[j...  51.9 us
    pallas_call x1, Pallas kernels, output_all(): pl.pallas_call(functools.partial(output_kernel, n), out_shape=jax.ShapeDt...  15.6 us
    reduce_sum x5, other arithmetic, rms_scale(): mean_square = jnp.mean(values * values, axis=-1, keepdims=True)  4.6 us

profile of v2, /device:TPU:1, one launch (start us, length us, event | category | flops | bytes accessed | tf_op | source)
XLA Modules:
  0.0 171.2 jit_solution(8686815858372319357)
XLA Ops:
  0.1 1.4 fusion.3
  1.5 0.8 slice_multiply_fusion.1
  2.2 0.7 dynamic_slice.11
  3.1 0.8 constant_dynamic-slice_fusion
  3.9 0.7 pad_maximum_fusion.1.refs_1_
  4.6 1.7 constant_dynamic-slice_fusion.1.refs_0_
  6.7 0.6 multiply_cosine_fusion
  8.1 1.0 copy.210
  9.0 61.5 %shard_map.199 = (bf16[160,192]{1,0:T(8,128)(2,1)}, bf16[160,144]{1,0:T(8,128)(2,1)}, bf16[160,256]{1,0:T(8,128)(2,1)}, bf16[160,256]{1,0:T(8,128)(2,1)}, bf16[1...) custom-call(bf16[2,4,160,256]{3,2,1,0:T(8,128)(2,1)} %bitcast.115, ...), custom_call_target="tpu_custom_call" | custom-call | tf_op jit(solution)/shard_map/pallas_call | solution.py:180
  70.5 1.3 fusion.45
  71.8 1.3 fusion.42
  73.2 1.2 fusion.56
  74.9 0.9 fusion.18
  75.8 0.9 fusion.17
  76.8 51.9 %shard_map.200 = (bf16[4,160,192]{2,1,0:T(8,128)(2,1)}, bf16[4,8,160,144]{3,2,1,0:T(8,128)(2,1)}, f32[8,2,256]{2,1,0:T(2,128)}, bf16[8,256,128]{2,1,0:T(8,128)(2...) custom-call(bf16[160,192]{1,0:T(8,128)(2,1)} %get-tuple-element.23.refs_0_, ...), custom_call_target="tpu_custom_call" | custom-call | tf_op jit(solution)/shard_map/pallas_call | solution.py:356
  128.7 0.8 fusion.98
  129.7 1.4 select_reduce_fusion.1
  131.1 1.1 fusion.25
  132.3 1.4 select_reduce_fusion
  133.8 1.7 multiply_reduce_fusion
  136.4 0.8 fusion.48
  139.2 0.8 subtract_convert_fusion.1
  140.6 1.6 slice_convert_fusion.1
  142.2 1.9 %copy.133 = f32[8,160,4,16]{1,0,3,2:T(8,128)} copy(f32[8,160,4,16]{3,1,0,2:T(8,128)S(1)} %slice_convert_fusion.1) | data formatting | bytes 655360 | tf_op jit(solution)/shard_map/convert_element_type | solution.py:564
  144.1 1.2 reshape.372
  145.4 1.6 slice_convert_fusion.2
  147.0 1.7 copy.129
  148.8 1.0 convolution_convert_fusion
  151.0 0.7 copy-done.6
  153.2 0.7 convert_element_type.213.attend_ref
  153.9 15.6 %shard_map.201 = f32[40,2048]{1,0:T(8,128)} custom-call(bf16[4,40,256]{2,1,0:T(8,128)(2,1)} %bitcast.116, bf16[4,40,256]{2,1,0:T(8,128)(2,1)} %convert_element_type.213.attend_ref, bf16[8,256,256]{2,1,0:T(8,128)(2,1)} %get-tuple-element.31.wc_ref, bf16[8,256,256]{2,1,0:T(8,128)(2,1)} %get-tuple-element.32.wa_ref), custom_call_target="tpu_custom_call" | custom-call | tf_op jit(solution)/shard_map/pallas_call | solution.py:418
  169.4 1.7 %copy.214 = f32[40,2048]{1,0:T(8,128)} copy(f32[40,2048]{1,0:T(8,128)} %shard_map.201) | data formatting | bytes 655360
  (82 shorter events, 8.3 us)
Async XLA Ops:
  0.0 138.1 %copy-start = (bf16[768,384]{1,0:T(8,128)(2,1)S(1)}, bf16[768,384]{1,0:T(8,128)(2,1)}, u32[]{:S(2)}) copy-start(bf16[768,384]{1,0:T(8,128)(2,1)} %param.35) | copy-start | bytes 1769476
  0.0 7.3 %copy-start.1 = (bf16[160,2048]{1,0:T(8,128)(2,1)S(1)}, bf16[160,2048]{1,0:T(8,128)(2,1)}, u32[]{:S(2)}) copy-start(bf16[160,2048]{1,0:T(8,128)(2,1)} %param.21) | copy-start | bytes 1966084
  0.0 7.3 %copy-start.9 = (f32[2048]{0:T(1024)S(1)}, f32[2048]{0:T(1024)}, u32[]{:S(2)}) copy-start(f32[2048]{0:T(1024)} %param.22) | copy-start | bytes 24580
  70.5 4.4 %copy-start.4 = (bf16[160,256]{1,0:T(8,128)(2,1)S(1)}, bf16[160,256]{1,0:T(8,128)(2,1)}, u32[]{:S(2)}) copy-start(bf16[160,256]{1,0:T(8,128)(2,1)} %get-tuple-element.19) | copy-start | bytes 245764
  132.2 4.2 %copy-start.5 = (bf16[160,256]{1,0:T(8,128)(2,1)S(1)}, bf16[160,256]{1,0:T(8,128)(2,1)}, u32[]{:S(2)}) copy-start(bf16[160,256]{1,0:T(8,128)(2,1)} %get-tuple-element.28) | copy-start | bytes 245764
  132.2 4.2 %copy-start.12 = (f32[256]{0:T(256)S(1)}, f32[256]{0:T(256)}, u32[]{:S(2)}) copy-start(f32[256]{0:T(256)} %param.29) | copy-start | bytes 3076
  132.3 4.8 %copy-start.2 = (bf16[4,160,192]{2,1,0:T(8,128)(2,1)S(1)}, bf16[4,160,192]{2,1,0:T(8,128)(2,1)}, u32[]{:S(2)}) copy-start(bf16[4,160,192]{2,1,0:T(8,128)(2,1)} %get-tuple-element.30) | copy-start | bytes 737284
  136.4 1.7 %copy-start.10 = (f32[768]{0:T(1024)S(1)}, f32[768]{0:T(1024)}, u32[]{:S(2)}) copy-start(f32[768]{0:T(1024)} %param.33) | copy-start | bytes 9220
  137.6 1.4 copy-start.13
  147.0 1.7 %copy-start.3 = (bf16[512,512]{1,0:T(8,128)(2,1)S(1)}, bf16[512,512]{1,0:T(8,128)(2,1)}, u32[]{:S(2)}) copy-start(bf16[512,512]{1,0:T(8,128)(2,1)} %param.36) | copy-start | bytes 1572868
  147.0 1.7 %copy-start.11 = (f32[512]{0:T(512)S(1)}, f32[512]{0:T(512)}, u32[]{:S(2)}) copy-start(f32[512]{0:T(512)} %param.34) | copy-start | bytes 6148
  149.9 0.7 copy-start.15
  150.8 0.9 copy-start.6
  150.8 0.9 copy-start.7
  150.8 1.0 copy-start.8
  152.3 0.7 copy-start.14

commit v3 on v2

--- a/solution.py
+++ b/solution.py
@@ -2,6 +2,7 @@
 
 import jax
 import jax.numpy as jnp
+import numpy as np
 from jax import lax
 from jax.experimental import pallas as pl
 from jax.experimental.pallas import tpu as pltpu
@@ -25,25 +26,6 @@
 def rms_scale(values, gain_vec):
     mean_square = jnp.mean(values * values, axis=-1, keepdims=True)
     return values * lax.rsqrt(mean_square + norm_eps) * gain_vec
-
-
-def rotate_tail(values, positions):
-    half_dim = ROPE_DIM // 2
-    inverse = rope_theta ** (-jnp.arange(0, ROPE_DIM, 2).astype(f32) / ROPE_DIM)
-    angles = positions.astype(f32)[:, None] * inverse
-    cosine = jnp.cos(angles)[:, None, :]
-    sine_table = jnp.sin(angles)[:, None, :]
-    unrotated = values[..., :NOPE_DIM]
-    first_half = values[..., NOPE_DIM : NOPE_DIM + half_dim]
-    latter = values[..., NOPE_DIM + half_dim :]
-    return jnp.concatenate(
-        [
-            unrotated,
-            first_half * cosine - latter * sine_table,
-            latter * cosine + first_half * sine_table,
-        ],
-        axis=-1,
-    )
 
 
 def greet(peers):
@@ -201,11 +183,42 @@
     )(x_split, *weights)
 
 
-def gather_kernel(n, heads_n, *refs):
+def heads_peer(n, d):
+    return {"tp": lax.rem(lax.axis_index("tp") + d, n)}
+
+
+def mixer_kernel(n, heads_n, *refs):
     count = 5
     query_in, pair_in, ins = refs[0], refs[1], refs[2 : 2 + count]
-    query_out, pair_out, outs = refs[2 + count], refs[3 + count], refs[4 + count : 4 + 2 * count]
-    keep, s1, r1, s2, r2, hs1, hr1, hs2, hr2 = refs[4 + 2 * count :]
+    (
+        fq_ref,
+        fk_ref,
+        bq_ref,
+        bk_ref,
+        v_ref,
+        gate_ref,
+        chain_gain_ref,
+        query_latent_gain_ref,
+        latent_gain_ref,
+        query_up_ref,
+        latent_up_ref,
+        query_gain_ref,
+        key_gain_ref,
+        mixer_gain_ref,
+        query_cos_ref,
+        query_sin_ref,
+        key_cos_ref,
+        key_sin_ref,
+        pick_key_ref,
+        swap_key_ref,
+        pick_plain_ref,
+        pick_query_ref,
+        swap_query_ref,
+        out_ref,
+    ) = refs[2 + count : 26 + count]
+    rest = refs[26 + count :]
+    query_out, pair_out, outs = rest[0], rest[1], rest[2 : 2 + count]
+    numer, denom, send, recv, keep, s1, r1, s2, r2, hs1, hr1, hs2, hr2, ss, rs = rest[2 + count :]
     me, lines, outer, inner, partner, line_peer = line_and_pair(n)
     head = lax.axis_index("tp")
     head_lines = heads_n // 2
@@ -216,9 +229,9 @@
         return {"tp": lax.rem(head_outer + d, head_lines) * 2 + head_inner}
 
     greet(
-        [partner, head_partner]
+        [partner]
         + [line_peer(d) for d in range(1, lines)]
-        + [head_peer(d) for d in range(1, head_lines)]
+        + [heads_peer(heads_n, d) for d in range(1, heads_n)]
     )
     src = (pair_in,) + tuple(ins)
 
@@ -322,114 +335,222 @@
     head_across(1, 0).start()
     for k in range(1, count - 1):
         pass_on(k)
+
+    rows, width = v_ref.shape
+    chain_heads = width // KEY_DIM
+
+    def lanes(h, size):
+        return slice(h * size, (h + 1) * size)
+
+    def against(a, b):
+        return lax.dot_general(a, b, (((1,), (1,)), ((), ())), preferred_element_type=f32)
+
+    row = lax.broadcasted_iota(jnp.int32, (rows, rows), 0)
+    col = lax.broadcasted_iota(jnp.int32, (rows, rows), 1)
+    within = []
+    for h in range(chain_heads):
+        at = lanes(h, KEY_DIM)
+        both = jnp.where(row >= col, against(fq_ref[:, at], fk_ref[:, at]), 0.0) + jnp.where(
+            row <= col, against(bq_ref[:, at], bk_ref[:, at]), 0.0
+        )
+        within.append(
+            jnp.dot(both.astype(bf16), v_ref[:, lanes(h, VAL_DIM)], preferred_element_type=f32)
+        )
+
     for d in range(1, head_lines):
         head_along(1, d).wait_recv()
         head_across(1, d).start()
-    for k in range(count - 1, 1 + count):
-        pass_on(k)
+    for k in (1, 2, 3):
+        local(k).wait()
+        across(k, 0).wait_recv()
+        on_line(k, False, lambda d: across(k, d).wait_recv())
+
+    log_ref, f_ref, b_ref = outs[0], outs[1], outs[2]
+
+    def forward(i, state):
+        return state * jnp.exp(log_ref[i, 0:1, :]) + f_ref[i].astype(f32)
+
+    def backward(i, state):
+        at = n - 1 - i
+        return state * jnp.exp(log_ref[at, 1:2, :]) + b_ref[at].astype(f32)
+
+    nothing = jnp.zeros(f_ref.shape[1:], f32)
+    f_in = lax.fori_loop(0, me, forward, nothing).astype(bf16)
+    b_in = lax.fori_loop(0, n - 1 - me, backward, nothing).astype(bf16)
+
+    def normed(values, size):
+        return lax.rsqrt(jnp.sum(values * values, axis=-1, keepdims=True) / size + norm_eps)
+
+    chain_parts = []
+    for h in range(chain_heads):
+        at = lanes(h, KEY_DIM)
+        total = (
+            within[h] + against(fq_ref[:, at], f_in[:, at]) + against(bq_ref[:, at], b_in[:, at])
+        )
+        gate = gate_ref[:, lanes(h, VAL_DIM)].astype(f32)
+        scaled = total * normed(total, VAL_DIM) * chain_gain_ref[:, lanes(h, VAL_DIM)]
+        chain_parts.append((scaled * (gate * jax.nn.sigmoid(gate))).astype(bf16))
+    chain_mixed = jnp.concatenate(chain_parts, axis=1)
+    pass_on(4)
 
     query_local.wait()
+    for j in range(head_lines):
+        head_across(0, j).wait_recv()
+    raws = [query_out[t].astype(f32) for t in range(heads_n)]
+    q_cols = raws[0].shape[1]
+    square = sum(jnp.sum(r * r, axis=-1, keepdims=True) for r in raws)
+    scale = lax.rsqrt(square / (heads_n * q_cols) + norm_eps)
+    attend_q = sum(
+        jnp.dot(
+            (raws[t] * scale * query_latent_gain_ref[t]).astype(bf16),
+            query_up_ref[t],
+            preferred_element_type=f32,
+        )
+        for t in range(heads_n)
+    ).astype(bf16)
+    heads = pick_plain_ref.shape[0]
+    q_plain, q_turned = [], []
+    for h in range(heads):
+        plain = jnp.dot(attend_q, pick_plain_ref[h], preferred_element_type=f32)
+        tail = jnp.dot(attend_q, pick_query_ref[h], preferred_element_type=f32)
+        swapped = jnp.dot(attend_q, swap_query_ref[h], preferred_element_type=f32)
+        square = jnp.sum(plain * plain, axis=-1, keepdims=True) + jnp.sum(
+            tail * tail, axis=-1, keepdims=True
+        )
+        scale = lax.rsqrt(square / ATT_QK + norm_eps)
+        q_plain.append((plain * scale * query_gain_ref[...]).astype(bf16))
+        q_turned.append(
+            ((tail * query_cos_ref[...] + swapped * query_sin_ref[...]) * scale).astype(bf16)
+        )
+
+    for d in range(head_lines):
+        head_across(1, d).wait_recv()
+    numer[...] = jnp.zeros_like(numer)
+    denom[...] = jnp.zeros_like(denom)
+    l_cols = latent_up_ref.shape[0] // heads_n
+
+    def attend(at, carry):
+        pieces = [pair_out[t, at] for t in range(heads_n)]
+        wide = [p[:, :l_cols].astype(f32) for p in pieces]
+        square = sum(jnp.sum(w * w, axis=-1, keepdims=True) for w in wide)
+        scale = lax.rsqrt(square / (heads_n * l_cols) + norm_eps)
+        latent = jnp.concatenate(
+            [
+                (wide[t] * scale * latent_gain_ref[:, lanes(t, l_cols)]).astype(bf16)
+                for t in range(heads_n)
+            ],
+            axis=1,
+        )
+        pairs = jnp.dot(latent, latent_up_ref[...], preferred_element_type=f32).astype(bf16)
+        tail = sum(
+            jnp.dot(pieces[t], pick_key_ref[t], preferred_element_type=f32)
+            for t in range(heads_n)
+        )
+        swapped = sum(
+            jnp.dot(pieces[t], swap_key_ref[t], preferred_element_type=f32)
+            for t in range(heads_n)
+        )
+        tail_square = jnp.sum(tail * tail, axis=-1, keepdims=True)
+        turned = tail * key_cos_ref[at] + swapped * key_sin_ref[at]
+        for h in range(heads):
+            start = h * (NOPE_DIM + VHEAD_DIM)
+            plain = pairs[:, start : start + NOPE_DIM].astype(f32)
+            value = pairs[:, start + NOPE_DIM : start + NOPE_DIM + VHEAD_DIM]
+            square = jnp.sum(plain * plain, axis=-1, keepdims=True) + tail_square
+            scale = lax.rsqrt(square / ATT_QK + norm_eps)
+            score = against(
+                q_plain[h], (plain * scale * key_gain_ref[...]).astype(bf16)
+            ) + against(q_turned[h], (turned * scale).astype(bf16))
+            weight = jnp.exp(score * ATT_QK ** (-0.5))
+            numer[h] += jnp.dot(weight.astype(bf16), value, preferred_element_type=f32)
+            denom[h] += jnp.sum(weight, axis=-1, keepdims=True)
+        return carry
+
+    lax.fori_loop(0, n // 2, attend, 0)
+    pass_on(5)
+    lax.fori_loop(n // 2, n, attend, 0)
+    attend_parts = []
+    for h in range(heads):
+        total = numer[h] / denom[h]
+        gain = mixer_gain_ref[:, lanes(h, VHEAD_DIM)]
+        attend_parts.append((total * normed(total, VHEAD_DIM) * gain).astype(bf16))
+    attend_mixed = jnp.concatenate(attend_parts, axis=1)
+
+    for k in (4, 5):
+        local(k).wait()
+        across(k, 0).wait_recv()
+        on_line(k, False, lambda d: across(k, d).wait_recv())
+    wc_ref, wa_ref = outs[3], outs[4]
+    col_n = wc_ref.shape[2]
+    part_rows = rows // heads_n
+    for i in range(n):
+        product = jnp.dot(chain_mixed, wc_ref[i], preferred_element_type=f32) + jnp.dot(
+            attend_mixed, wa_ref[i], preferred_element_type=f32
+        )
+        for t in range(heads_n):
+            send[t, :, lanes(i, col_n)] = product[lanes(t, part_rows)].astype(bf16)
+
+    def sum_copy(d):
+        return pltpu.make_async_remote_copy(
+            src_ref=send.at[lax.rem(head + d, heads_n)],
+            dst_ref=recv.at[d],
+            send_sem=ss.at[d],
+            recv_sem=rs.at[d],
+            device_id=heads_peer(heads_n, d),
+            device_id_type=MESH,
+        )
+
+    for d in range(1, heads_n):
+        sum_copy(d).start()
+    total = send[head].astype(f32)
+    for d in range(1, heads_n):
+        sum_copy(d).wait_recv()
+        total = total + recv[d].astype(f32)
+    out_ref[...] = total
+
+    for d in range(1, heads_n):
+        sum_copy(d).wait_send()
     for k in range(1 + count):
         across(k, 0).wait_send()
-        if k > 0:
-            local(k).wait()
-            across(k, 0).wait_recv()
         on_line(k, True, lambda d: along(k, d).wait_send())
-
-        def act(d):
-            across(k, d).wait_send()
-            if k > 0:
-                across(k, d).wait_recv()
-
-        on_line(k, False, act)
+        on_line(k, False, lambda d: across(k, d).wait_send())
     for j in range(2):
-        head_across(j, 0).wait()
+        head_across(j, 0).wait_send()
         for d in range(1, head_lines):
             head_along(j, d).wait_send()
-            head_across(j, d).wait()
-
-
-def gather_all(n, heads_n, query, pair, blocks):
+            head_across(j, d).wait_send()
+
+
+def mix_all(n, heads_n, query, pair, blocks, others, heads):
     lines, head_lines = n // 2, heads_n // 2
     count = len(blocks)
+    rows = query.shape[0]
+    out_cols = n * blocks[-1].shape[1]
     vmem = pl.BlockSpec(memory_space=pltpu.VMEM)
     return pl.pallas_call(
-        functools.partial(gather_kernel, n, heads_n),
-        out_shape=[
-            jax.ShapeDtypeStruct((heads_n,) + query.shape, query.dtype),
-            jax.ShapeDtypeStruct((heads_n, n) + pair.shape, pair.dtype),
+        functools.partial(mixer_kernel, n, heads_n),
+        out_shape=jax.ShapeDtypeStruct((rows // heads_n, out_cols), f32),
+        in_specs=[vmem] * (2 + count + len(others)),
+        out_specs=vmem,
+        scratch_shapes=[
+            pltpu.VMEM((heads_n,) + query.shape, query.dtype),
+            pltpu.VMEM((heads_n, n) + pair.shape, pair.dtype),
         ]
-        + [jax.ShapeDtypeStruct((n,) + b.shape, b.dtype) for b in blocks],
-        in_specs=[vmem] * (2 + count),
-        out_specs=[vmem] * (2 + count),
-        scratch_shapes=[pltpu.SemaphoreType.DMA((2 + count,))]
+        + [pltpu.VMEM((n,) + b.shape, b.dtype) for b in blocks]
+        + [
+            pltpu.VMEM((heads, rows, VHEAD_DIM), f32),
+            pltpu.VMEM((heads, rows, 1), f32),
+            pltpu.VMEM((heads_n, rows // heads_n, out_cols), bf16),
+            pltpu.VMEM((heads_n, rows // heads_n, out_cols), bf16),
+            pltpu.SemaphoreType.DMA((2 + count,)),
+        ]
         + [pltpu.SemaphoreType.DMA((1 + count, lines))] * 4
-        + [pltpu.SemaphoreType.DMA((2, head_lines))] * 4,
+        + [pltpu.SemaphoreType.DMA((2, head_lines))] * 4
+        + [pltpu.SemaphoreType.DMA((heads_n,))] * 2,
         compiler_params=pltpu.CompilerParams(
             collective_id=1, has_side_effects=True, vmem_limit_bytes=VMEM_LIMIT
         ),
-    )(query, pair, *blocks)
-
-
-def heads_peer(n, d):
-    return {"tp": lax.rem(lax.axis_index("tp") + d, n)}
-
-
-def output_kernel(n, chain_ref, attend_ref, wc_ref, wa_ref, out_ref, send, recv, ss, rs):
-    me = lax.axis_index("tp")
-    greet([heads_peer(n, d) for d in range(1, n)])
-
-    def copy(d):
-        return pltpu.make_async_remote_copy(
-            src_ref=send.at[d],
-            dst_ref=recv.at[d],
-            send_sem=ss.at[d],
-            recv_sem=rs.at[d],
-            device_id=heads_peer(n, d),
-            device_id_type=MESH,
-        )
-
-    def rows_of(at):
-        chain, attend = chain_ref[at], attend_ref[at]
-        return jnp.concatenate(
-            [
-                jnp.dot(chain, wc_ref[s], preferred_element_type=f32)
-                + jnp.dot(attend, wa_ref[s], preferred_element_type=f32)
-                for s in range(wc_ref.shape[0])
-            ],
-            axis=1,
-        )
-
-    for d in range(1, n):
-        send[d] = rows_of(lax.rem(me + d, n)).astype(bf16)
-        copy(d).start()
-    total = rows_of(me)
-    for d in range(1, n):
-        copy(d).wait_recv()
-        total = total + recv[d].astype(f32)
-    out_ref[...] = total
-    for d in range(1, n):
-        copy(d).wait_send()
-
-
-def output_all(n, chain, attend, chain_w, attend_w):
-    rows, cols = chain.shape[1], chain_w.shape[0] * chain_w.shape[2]
-    vmem = pl.BlockSpec(memory_space=pltpu.VMEM)
-    return pl.pallas_call(
-        functools.partial(output_kernel, n),
-        out_shape=jax.ShapeDtypeStruct((rows, cols), f32),
-        in_specs=[vmem] * 4,
-        out_specs=vmem,
-        scratch_shapes=[
-            pltpu.VMEM((n, rows, cols), bf16),
-            pltpu.VMEM((n, rows, cols), bf16),
-            pltpu.SemaphoreType.DMA((n,)),
-            pltpu.SemaphoreType.DMA((n,)),
-        ],
-        compiler_params=pltpu.CompilerParams(
-            collective_id=3, has_side_effects=True, vmem_limit_bytes=VMEM_LIMIT
-        ),
-    )(chain, attend, chain_w, attend_w)
+    )(query, pair, *blocks, *others)
 
 
 def gate_parts(pre_gate, rate_row, seq_len):
@@ -483,9 +604,6 @@
         (q_down, l_down, chain_query, forward_gate, backward_gate, chain_value, output_gate),
     )
 
-    def project(source, weight):
-        return jnp.dot(source, weight, preferred_element_type=f32).astype(bf16)
-
     f_log, f_key = gate_parts(fwd_logit, forget_rate[0], seq_len)
     b_log, b_key = gate_parts(bwd_logit, forget_rate[1], seq_len)
     width = f_log.shape[1]
@@ -495,108 +613,85 @@
     b_cum = jnp.dot(lower.T, b_log, precision=lax.Precision.HIGHEST)
     q_wide = q_rows.astype(f32)
 
-    def by_head(tensor):
-        return tensor.astype(bf16).reshape(rows, chain_heads, -1)
-
-    f_q, f_k = by_head(q_wide * jnp.exp(f_cum)), by_head(f_key * jnp.exp(-f_cum))
-    b_q, b_k = by_head(q_wide * jnp.exp(b_cum)), by_head(b_key * jnp.exp(-b_cum))
-    v_heads = v_rows.reshape(rows, chain_heads, VAL_DIM)
+    f_q, f_k = (q_wide * jnp.exp(f_cum)).astype(bf16), (f_key * jnp.exp(-f_cum)).astype(bf16)
+    b_q, b_k = (q_wide * jnp.exp(b_cum)).astype(bf16), (b_key * jnp.exp(-b_cum)).astype(bf16)
     logs = jnp.stack([f_cum[-1], b_cum[0]])
 
     def digest(keys, log):
-        state = jnp.einsum("jre,jrw->rew", keys, v_heads, preferred_element_type=f32)
-        return state * jnp.exp(log).reshape(chain_heads, KEY_DIM, 1)
-
-    f_state, b_state = digest(f_k, logs[0]).astype(bf16), digest(b_k, logs[1]).astype(bf16)
-
-    query_raw, pair_raw, all_logs, all_f, all_b, all_chain, all_attend = gather_all(
+        parts = [
+            lax.dot_general(
+                v_rows[:, h * VAL_DIM : (h + 1) * VAL_DIM],
+                keys[:, h * KEY_DIM : (h + 1) * KEY_DIM],
+                (((0,), (0,)), ((), ())),
+                preferred_element_type=f32,
+            )
+            for h in range(chain_heads)
+        ]
+        return (jnp.concatenate(parts, axis=1) * jnp.exp(log)).astype(bf16)
+
+    heads = query_up.shape[1] // ATT_QK
+    half = ROPE_DIM // 2
+    inverse = rope_theta ** (-jnp.arange(0, ROPE_DIM, 2).astype(f32) / ROPE_DIM)
+    angles = jnp.arange(seq_len, dtype=jnp.int32).astype(f32)[:, None] * inverse
+    cosine = jnp.tile(jnp.cos(angles), (1, 2))
+    sine = jnp.tile(jnp.sin(angles), (1, 2))
+
+    def tables(gain, cos_rows, sin_rows):
+        tail = gain[NOPE_DIM:]
+        return cos_rows * tail, sin_rows * jnp.roll(tail, half)
+
+    own_rows = functools.partial(
+        lax.dynamic_slice_in_dim, start_index=sp * rows, slice_size=rows, axis=0
+    )
+    query_tables = tables(query_head_gain, own_rows(cosine), own_rows(sine))
+    key_tables = [
+        t.reshape(n_sp, rows, ROPE_DIM) for t in tables(key_head_gain, cosine, sine)
+    ]
+    swap = np.zeros((ROPE_DIM, ROPE_DIM), np.float32)
+    for j in range(half):
+        swap[half + j, j] = -1.0
+        swap[j, half + j] = 1.0
+    pick_key = np.zeros((n_tp, l_cols + r_cols, ROPE_DIM), np.float32)
+    for t in range(n_tp):
+        for j in range(r_cols):
+            pick_key[t, l_cols + j, t * r_cols + j] = 1.0
+    pick_plain = np.zeros((heads, heads * ATT_QK, NOPE_DIM), np.float32)
+    pick_query = np.zeros((heads, heads * ATT_QK, ROPE_DIM), np.float32)
+    for h in range(heads):
+        for j in range(NOPE_DIM):
+            pick_plain[h, h * ATT_QK + j, j] = 1.0
+        for j in range(ROPE_DIM):
+            pick_query[h, h * ATT_QK + NOPE_DIM + j, j] = 1.0
+    picks = [
+        jnp.asarray(p, bf16)
+        for p in (pick_key, pick_key @ swap, pick_plain, pick_query, pick_query @ swap)
+    ]
+    return mix_all(
         n_sp,
         n_tp,
         raw_q,
         raw_l,
+        (logs, digest(f_k, logs[0]), digest(b_k, logs[1]), chain_out, attend_out),
         (
-            logs,
-            f_state.reshape(width, VAL_DIM),
-            b_state.reshape(width, VAL_DIM),
-            chain_out,
-            attend_out,
+            f_q,
+            f_k,
+            b_q,
+            b_k,
+            v_rows,
+            gate_logit,
+            chain_gain[None],
+            query_latent_gain.reshape(n_tp, 1, q_cols),
+            latent_gain[None],
+            query_up.reshape(n_tp, q_cols, -1),
+            latent_up,
+            query_head_gain[None, :NOPE_DIM],
+            key_head_gain[None, :NOPE_DIM],
+            mixer_gain[None],
+            *query_tables,
+            *key_tables,
+            *picks,
         ),
-    )
-
-    index = jnp.arange(n_sp)
-    before = (index < sp)[:, None]
-    after = (index > sp)[:, None]
-    between_f = ((index[None, :] > index[:, None]) & (index[None, :] < sp)).astype(f32)
-    between_b = ((index[None, :] < index[:, None]) & (index[None, :] > sp)).astype(f32)
-    sum_f = jnp.sum(between_f[:, :, None] * all_logs[None, :, 0], axis=1)
-    sum_b = jnp.sum(between_b[:, :, None] * all_logs[None, :, 1], axis=1)
-    def entering(mask, log_sum, states):
-        wide = jnp.exp(log_sum)[:, :, None] * states.astype(f32)
-        total = jnp.sum(jnp.where(mask[:, :, None], wide, 0.0), axis=0)
-        return total.astype(bf16).reshape(chain_heads, KEY_DIM, VAL_DIM)
-
-    f_in, b_in = entering(before, sum_f, all_f), entering(after, sum_b, all_b)
-
-    def scores(queries, keys, mask):
-        return (
-            jnp.einsum("thk,shk->hts", queries, keys, preferred_element_type=f32) * mask
-        )
-
-    both = (scores(f_q, f_k, lower) + scores(b_q, b_k, lower.T)).astype(bf16)
-    combined = (
-        jnp.einsum("hts,shv->thv", both, v_heads, preferred_element_type=f32)
-        + jnp.einsum("thk,hkv->thv", f_q, f_in, preferred_element_type=f32)
-        + jnp.einsum("thk,hkv->thv", b_q, b_in, preferred_element_type=f32)
-    )
-    head_gain = chain_gain.reshape(chain_heads, VAL_DIM)
-    chain_mixed = (
-        rms_scale(combined, head_gain).reshape(rows, -1) * jax.nn.silu(gate_logit.astype(f32))
-    ).astype(bf16)
-
-    heads = query_up.shape[1] // ATT_QK
-    query_latent = rms_scale(
-        query_raw.transpose(1, 0, 2).reshape(rows, -1).astype(f32), query_latent_gain
-    ).astype(bf16)
-    pair_rows = pair_raw.transpose(1, 2, 0, 3)
-    pair_latent = rms_scale(
-        pair_rows[..., :l_cols].reshape(seq_len, -1).astype(f32), latent_gain
-    ).astype(bf16)
-    rotary_key = pair_rows[..., l_cols:].reshape(seq_len, ROPE_DIM).astype(f32)
-    attend_query = project(query_latent, query_up).astype(f32).reshape(rows, heads, ATT_QK)
-    attend_pairs = project(pair_latent, latent_up).reshape(seq_len, heads, NOPE_DIM + VHEAD_DIM)
-    query_final = rotate_tail(
-        rms_scale(attend_query, query_head_gain), sp * rows + jnp.arange(rows, dtype=jnp.int32)
-    ).astype(bf16)
-    key_cat = jnp.concatenate(
-        [
-            attend_pairs[..., :NOPE_DIM].astype(f32),
-            jnp.broadcast_to(rotary_key[:, None, :], (seq_len, heads, ROPE_DIM)),
-        ],
-        axis=-1,
-    )
-    key_all = rotate_tail(
-        rms_scale(key_cat, key_head_gain), jnp.arange(seq_len, dtype=jnp.int32)
-    ).astype(bf16)
-    value_all = attend_pairs[..., NOPE_DIM:]
-    weights = jnp.exp(
-        jnp.einsum("qhd,khd->hqk", query_final, key_all, preferred_element_type=f32)
-        * ATT_QK ** (-0.5)
-    )
-    numerator = jnp.einsum(
-        "hqk,khv->qhv", weights.astype(bf16), value_all, preferred_element_type=f32
-    )
-    denominator = jnp.sum(weights, axis=-1)
-    attend_rows = numerator / jnp.transpose(denominator)[:, :, None]
-    attend_mixed = (
-        rms_scale(attend_rows, mixer_gain.reshape(heads, VHEAD_DIM))
-        .reshape(rows, heads * VHEAD_DIM)
-        .astype(bf16)
-    )
-    def row_blocks(tensor):
-        return tensor.reshape(n_tp, rows // n_tp, -1)
-
-    return output_all(
-        n_tp, row_blocks(chain_mixed), row_blocks(attend_mixed), all_chain, all_attend
+        heads,
     )
 
 

time: 172 us -> 146 us (0.85)
  other arithmetic: 17.6 us -> 6.31 us
  local copies, waits for them, and re-layouts: 16.3 us -> 9.43 us
  matrix products: 7.78 us -> 3.22 us
  Pallas kernels: 129 us -> 127 us
    convert_element_type x7 -> x0, local copies, waits for them, and re-layouts: 6.46 us -> none  [the longest x2 3.19 us: on_device(): rotary_key = pair_rows[..., l_cols:].reshape(seq_len, ROPE_DIM).astype(f32)]
    dot_general x10 -> x4, matrix products: 5.18 us -> 0.75 us  [digest(): lax.dot_general(v_rows[:, h * VAL_DIM:(h + 1) * VAL_DIM], keys[:, h * KEY...]
    reduce_sum x5 -> x1, other arithmetic: 4.6 us -> 0.21 us  [rms_scale(): mean_square = jnp.mean(values * values, axis=-1, keepdims=True)]
    reduce_sum x4 -> x0, other arithmetic: 3 us -> none  [the longest x2 2.82 us: entering(): total = jnp.sum(jnp.where(mask[:, :, None], wide, 0.0), axis=0)]
    convert_element_type x10 -> x3, other arithmetic: 4.24 us -> 1.29 us  [the longest x2 1.28 us: digest(): return (jnp.concatenate(parts, axis=1) * jnp.exp(log)).astype(bf16)]
    pallas_call x2 -> x1, Pallas kernels: 67.5 us -> 65.3 us  [mix_all(): pl.pallas_call(functools.partial(mixer_kernel, n, heads_n), out_shape=jax...]
    mul x2 -> x3, other arithmetic: 0.35 us -> 2.49 us  [tables(): return (cos_rows * tail, sin_rows * jnp.roll(tail, half))]
where the time goes in v3:
time: 146 us
  Pallas kernels  127 us (87%)
  local copies, waits for them, and re-layouts  9.43 us (6%)
  other arithmetic  6.31 us (4%)
  matrix products  3.22 us (2%)
    pallas_call x1, Pallas kernels, mix_all(): pl.pallas_call(functools.partial(mixer_kernel, n, heads_n), out_shape=jax...  65.3 us
    pallas_call x1, Pallas kernels, project_all(): pl.pallas_call(functools.partial(project_kernel, n, count), out_shape=[ja...  61.5 us

profile of v3, /device:TPU:1, one launch (start us, length us, event | category | flops | bytes accessed | tf_op | source)
XLA Modules:
  0.0 146.0 jit_solution(3019990416386837989)
XLA Ops:
  0.0 0.8 dynamic_slice.17
  0.9 0.9 constant_dynamic-slice_fusion.2
  1.8 0.7 pad_maximum_fusion.refs_1_
  2.5 0.8 constant_dynamic-slice_fusion.3.refs_0_
  3.2 0.2 fusion
  3.5 0.2 fusion.2
  3.7 0.5 reshape.109
  4.2 1.0 copy.62
  5.1 61.5 %shard_map.244 = (bf16[160,192]{1,0:T(8,128)(2,1)}, bf16[160,144]{1,0:T(8,128)(2,1)}, bf16[160,256]{1,0:T(8,128)(2,1)}, bf16[160,256]{1,0:T(8,128)(2,1)}, bf16[1...) custom-call(bf16[2,4,160,256]{3,2,1,0:T(8,128)(2,1)} %bitcast.21, ...), custom_call_target="tpu_custom_call" | custom-call | tf_op jit(solution)/shard_map/pallas_call | solution.py:162
  66.7 1.3 fusion.5
  68.1 1.1 fusion.8
  69.2 0.2 fusion.21
  69.4 0.2 fusion.19
  69.6 0.6 fusion.14.refs_4_
  70.3 0.2 fusion.25
  70.4 0.2 fusion.23
  70.6 0.6 fusion.13.refs_3_
  71.3 0.6 pad_maximum_fusion.1.refs_2_
  71.9 0.6 multiply_sine_fusion
  72.9 0.4 copy-done.8
  73.4 0.6 broadcast_multiply_fusion.2.refs_22_
  74.1 0.6 broadcast_multiply_fusion.3.refs_21_
  74.8 0.3 tile.30
  75.1 0.3 copy.50
  75.4 0.3 tile.31
  75.7 0.3 copy.52
  76.0 0.4 copy-done.7
  76.5 1.2 broadcast_multiply_fusion
  77.7 0.6 slice_bitcast_fusion
  78.3 0.7 reshape.110.refs_14_
  79.0 65.3 %shard_map.245 = f32[40,2048]{1,0:T(8,128)} custom-call(bf16[160,192]{1,0:T(8,128)(2,1)} %get-tuple-element.12.refs_0_, bf16[160,144]{1,0:T(8,128)(2,1)} %get-tuple-element.13.refs_1_, f32[2,256]{1,0:T(2,128)} %pad_maximum_fusion.1.refs_2_, bf16[128,256]{1,0:T(8,128)(2,1)} %fusion.13.refs_3_, bf16[128,256]{1,0:T(8,128)(2,1)} %fusion.14.refs_4_, ...), custom_call_target="tpu_custom_call" | custom-call | tf_op jit(solution)/shard_map/pallas_call | solution.py:530
  144.3 1.7 %copy.64 = f32[40,2048]{1,0:T(8,128)} copy(f32[40,2048]{1,0:T(8,128)} %shard_map.245) | data formatting | bytes 655360
  (41 shorter events, 0.9 us)
Async XLA Ops:
  0.0 2.5 %copy-start = (bf16[256,768]{1,0:T(8,128)(2,1)S(1)}, bf16[256,768]{1,0:T(8,128)(2,1)}, u32[]{:S(2)}) copy-start(bf16[256,768]{1,0:T(8,128)(2,1)} %param.35) | copy-start | bytes 1179652
  0.0 3.2 %copy-start.1 = (bf16[160,2048]{1,0:T(8,128)(2,1)S(1)}, bf16[160,2048]{1,0:T(8,128)(2,1)}, u32[]{:S(2)}) copy-start(bf16[160,2048]{1,0:T(8,128)(2,1)} %param.26) | copy-start | bytes 1966084
  0.9 2.5 %copy-start.5 = (f32[2048]{0:T(1024)S(1)}, f32[2048]{0:T(1024)}, u32[]{:S(2)}) copy-start(f32[2048]{0:T(1024)} %param.27) | copy-start | bytes 24580
  5.1 61.5 %copy-start.9 = (f32[2,256]{1,0:T(2,128)S(1)}, f32[2,256]{1,0:T(2,128)}, u32[]{:S(2)}) copy-start(f32[2,256]{1,0:T(2,128)} %param.33) | copy-start | bytes 6148
  66.6 1.4 copy-start.10
  66.6 1.4 copy-start.11
  66.6 1.4 copy-start.12
  68.0 1.2 copy-start.2
  69.2 3.4 %copy-start.3 = (bf16[160,256]{1,0:T(8,128)(2,1)}, bf16[160,256]{1,0:T(8,128)(2,1)S(1)}, u32[]{:S(2)}) copy-start(bf16[160,256]{1,0:T(8,128)(2,1)S(1)} %get-tuple-element.20.refs_10_) | copy-start | bytes 245764
  69.2 3.4 %copy-start.4 = (bf16[160,256]{1,0:T(8,128)(2,1)}, bf16[160,256]{1,0:T(8,128)(2,1)S(1)}, u32[]{:S(2)}) copy-start(bf16[160,256]{1,0:T(8,128)(2,1)S(1)} %get-tuple-element.27.refs_8_) | copy-start | bytes 245764
  72.6 0.7 copy-start.8
  75.7 0.7 copy-start.7
  76.5 1.8 %copy-start.6 = (f32[768]{0:T(1024)S(1)}, f32[768]{0:T(1024)}, u32[]{:S(2)}) copy-start(f32[768]{0:T(1024)} %param.38) | copy-start | bytes 9220

commit v4 on v3

--- a/solution.py
+++ b/solution.py
@@ -23,11 +23,6 @@
 bf16 = jnp.bfloat16
 
 
-def rms_scale(values, gain_vec):
-    mean_square = jnp.mean(values * values, axis=-1, keepdims=True)
-    return values * lax.rsqrt(mean_square + norm_eps) * gain_vec
-
-
 def greet(peers):
     barrier = pltpu.get_barrier_semaphore()
     for peer in peers:
@@ -47,16 +42,29 @@
     return me, lines, outer, inner, partner, line_peer
 
 
-def project_kernel(n, count, x_ref, *refs):
-    weights = refs[:count]
-    outs = refs[count : 2 * count]
-    rest = refs[2 * count :]
-    x_recv = rest[0]
-    w_recv = rest[1 : 1 + count]
-    p_send = rest[1 + count : 1 + 2 * count]
-    p_recv = rest[1 + 2 * count : 1 + 3 * count]
-    own = rest[1 + 3 * count : 1 + 4 * count]
-    xs, xr, ws, wr, ps, pr = rest[1 + 4 * count :]
+def project_kernel(n, count, *refs):
+    tokens_ref, gain_ref, rate_ref = refs[:3]
+    weights = refs[3 : 3 + count]
+    (
+        v_ref,
+        gate_ref,
+        ql_ref,
+        ll_ref,
+        fq_ref,
+        fk_ref,
+        bq_ref,
+        bk_ref,
+        log_ref,
+        f_state_ref,
+        b_state_ref,
+    ) = refs[3 + count : 14 + count]
+    rest = refs[14 + count :]
+    x_ref, x_recv = rest[0], rest[1]
+    w_recv = rest[2 : 2 + count]
+    p_send = rest[2 + count : 2 + 2 * count]
+    p_recv = rest[2 + 2 * count : 2 + 3 * count]
+    own = rest[2 + 3 * count : 2 + 4 * count]
+    xs, xr, ws, wr, ps, pr = rest[2 + 4 * count :]
     groups = n // 4
     me = lax.axis_index("sp")
     group, place = me // 4, lax.rem(me, 4)
@@ -107,6 +115,14 @@
 
     w_copy(0, 0).start()
     w_copy(0, 1).start()
+    wide = tokens_ref[...].astype(f32)
+    scale = lax.rsqrt(jnp.mean(wide * wide, axis=-1, keepdims=True) + norm_eps)
+    normed = (wide * scale * gain_ref[...]).astype(bf16)
+    rows, depth = x_ref.shape[2:]
+    for g in range(groups):
+        for k in range(4):
+            first = (g * 4 + k) * depth
+            x_ref[g, k] = normed[:, first : first + depth]
     for d in range(1, groups):
         x_copy(d).start()
     for c in range(1, count):
@@ -116,6 +132,51 @@
         w_copy(c, 2).start()
         if c + 1 < count:
             w_copy(c + 1, 1).start()
+    def finished(c):
+        def add(d, total):
+            p_copy(c, d).wait_recv()
+            return total + p_recv[c][d].astype(f32)
+
+        return lax.fori_loop(1, groups, add, own[c][...]).astype(bf16)
+
+    def recurrence():
+        value = finished(0)
+        v_ref[...] = value
+        row = lax.broadcasted_iota(jnp.int32, (rows, rows), 0)
+        col = lax.broadcasted_iota(jnp.int32, (rows, rows), 1)
+
+        def direction(c, mask, last):
+            rate = rate_ref[c - 1 : c, :] / (rows * n)
+            key = rate * jax.nn.sigmoid(-finished(c).astype(f32))
+            total = jnp.dot(
+                jnp.where(mask, 1.0, 0.0),
+                jnp.log1p(-key),
+                precision=lax.Precision.HIGHEST,
+                preferred_element_type=f32,
+            )
+            full = total[last : last + 1, :]
+            key = (key * jnp.exp(-total)).astype(bf16)
+            state = jnp.concatenate(
+                [
+                    lax.dot_general(
+                        value[:, h * VAL_DIM : (h + 1) * VAL_DIM],
+                        key[:, h * KEY_DIM : (h + 1) * KEY_DIM],
+                        (((0,), (0,)), ((), ())),
+                        preferred_element_type=f32,
+                    )
+                    for h in range(value.shape[1] // VAL_DIM)
+                ],
+                axis=1,
+            )
+            log_ref[c - 1 : c, :] = full
+            return key, total, (state * jnp.exp(full)).astype(bf16)
+
+        fk_ref[...], f_total, f_state_ref[...] = direction(1, row >= col, rows - 1)
+        bk_ref[...], b_total, b_state_ref[...] = direction(2, row <= col, 0)
+        query = finished(3).astype(f32)
+        fq_ref[...] = (query * jnp.exp(f_total)).astype(bf16)
+        bq_ref[...] = (query * jnp.exp(b_total)).astype(bf16)
+
     for c in range(count):
         w_copy(c, 1).wait_recv()
         w_copy(c, 2).wait_recv()
@@ -135,13 +196,11 @@
             p_copy(c, back).start()
 
         own[c][...] = part(lambda k: x_ref[group, k])
-    for c in range(count):
-
-        def add(d, total):
-            p_copy(c, d).wait_recv()
-            return total + p_recv[c][d].astype(f32)
-
-        outs[c][...] = lax.fori_loop(1, groups, add, own[c][...]).astype(bf16)
+        if c == count - 2:
+            recurrence()
+    gate_ref[...] = finished(4)
+    ql_ref[...] = finished(5)
+    ll_ref[...] = finished(6)
     for d in range(1, groups):
         x_copy(d).wait_send()
     for c in range(count):
@@ -153,18 +212,23 @@
             p_copy(c, d).wait_send()
 
 
-def project_all(n, x_split, weights):
+def project_all(n, tokens, gain, rates, weights):
     groups = n // 4
-    rows, depth = x_split.shape[2:]
+    rows, depth = tokens.shape[0], weights[0].shape[0]
     count = len(weights)
     widths = [w.shape[1] for w in weights]
+    width = widths[0]
+    wide = jax.ShapeDtypeStruct((rows, width), bf16)
+    state = jax.ShapeDtypeStruct((VAL_DIM, width), bf16)
     vmem = pl.BlockSpec(memory_space=pltpu.VMEM)
     return pl.pallas_call(
         functools.partial(project_kernel, n, count),
-        out_shape=[jax.ShapeDtypeStruct((rows, c), bf16) for c in widths],
-        in_specs=[vmem] * (1 + count),
-        out_specs=[vmem] * count,
-        scratch_shapes=[pltpu.VMEM((groups, 4, rows, depth), bf16)]
+        out_shape=[jax.ShapeDtypeStruct((rows, widths[c]), bf16) for c in (0, 4, 5, 6)]
+        + [wide] * 4
+        + [jax.ShapeDtypeStruct((2, width), f32), state, state],
+        in_specs=[vmem] * (3 + count),
+        out_specs=[vmem] * 11,
+        scratch_shapes=[pltpu.VMEM((groups, 4, rows, depth), bf16)] * 2
         + [pltpu.VMEM((3, depth, c), bf16) for c in widths]
         + [pltpu.VMEM((groups, rows, c), bf16) for c in widths]
         + [pltpu.VMEM((groups, rows, c), bf16) for c in widths]
@@ -180,7 +244,7 @@
         compiler_params=pltpu.CompilerParams(
             collective_id=0, has_side_effects=True, vmem_limit_bytes=VMEM_LIMIT
         ),
-    )(x_split, *weights)
+    )(tokens, gain, rates, *weights)
 
 
 def heads_peer(n, d):
@@ -205,10 +269,10 @@
         query_gain_ref,
         key_gain_ref,
         mixer_gain_ref,
-        query_cos_ref,
-        query_sin_ref,
-        key_cos_ref,
-        key_sin_ref,
+        query_tail_ref,
+        key_tail_ref,
+        cos_ref,
+        sin_ref,
         pick_key_ref,
         swap_key_ref,
         pick_plain_ref,
@@ -403,12 +467,14 @@
     attend_q = sum(
         jnp.dot(
             (raws[t] * scale * query_latent_gain_ref[t]).astype(bf16),
-            query_up_ref[t],
+            query_up_ref[lanes(t, q_cols), :],
             preferred_element_type=f32,
         )
         for t in range(heads_n)
     ).astype(bf16)
     heads = pick_plain_ref.shape[0]
+    query_cos = cos_ref[me] * query_tail_ref[0:1, :]
+    query_sin = sin_ref[me] * query_tail_ref[1:2, :]
     q_plain, q_turned = [], []
     for h in range(heads):
         plain = jnp.dot(attend_q, pick_plain_ref[h], preferred_element_type=f32)
@@ -420,7 +486,7 @@
         scale = lax.rsqrt(square / ATT_QK + norm_eps)
         q_plain.append((plain * scale * query_gain_ref[...]).astype(bf16))
         q_turned.append(
-            ((tail * query_cos_ref[...] + swapped * query_sin_ref[...]) * scale).astype(bf16)
+            ((tail * query_cos + swapped * query_sin) * scale).astype(bf16)
         )
 
     for d in range(head_lines):
@@ -451,7 +517,9 @@
             for t in range(heads_n)
         )
         tail_square = jnp.sum(tail * tail, axis=-1, keepdims=True)
-        turned = tail * key_cos_ref[at] + swapped * key_sin_ref[at]
+        turned = (tail * key_tail_ref[0:1, :]) * cos_ref[at] + (
+            swapped * key_tail_ref[1:2, :]
+        ) * sin_ref[at]
         for h in range(heads):
             start = h * (NOPE_DIM + VHEAD_DIM)
             plain = pairs[:, start : start + NOPE_DIM].astype(f32)
@@ -551,11 +619,6 @@
             collective_id=1, has_side_effects=True, vmem_limit_bytes=VMEM_LIMIT
         ),
     )(query, pair, *blocks, *others)
-
-
-def gate_parts(pre_gate, rate_row, seq_len):
-    opening = rate_row / seq_len * jax.nn.sigmoid(-pre_gate.astype(f32))
-    return (jnp.log1p(-opening), opening)
 
 
 def on_device(
@@ -596,57 +659,27 @@
         ],
         axis=1,
     )
-    normed = rms_scale(tokens.astype(f32), input_gain).astype(bf16)
-    x_split = normed.reshape(rows, n_sp // 4, 4, depth).transpose(1, 2, 0, 3)
-    raw_q, raw_l, q_rows, fwd_logit, bwd_logit, v_rows, gate_logit = project_all(
+    (v_rows, gate_logit, raw_q, raw_l, f_q, f_k, b_q, b_k, logs, f_state, b_state) = project_all(
         n_sp,
-        x_split,
-        (q_down, l_down, chain_query, forward_gate, backward_gate, chain_value, output_gate),
+        tokens,
+        input_gain[None],
+        forget_rate,
+        (chain_value, forward_gate, backward_gate, chain_query, output_gate, q_down, l_down),
     )
-
-    f_log, f_key = gate_parts(fwd_logit, forget_rate[0], seq_len)
-    b_log, b_key = gate_parts(bwd_logit, forget_rate[1], seq_len)
-    width = f_log.shape[1]
-    chain_heads = width // KEY_DIM
-    lower = jnp.tril(jnp.ones((rows, rows), f32))
-    f_cum = jnp.dot(lower, f_log, precision=lax.Precision.HIGHEST)
-    b_cum = jnp.dot(lower.T, b_log, precision=lax.Precision.HIGHEST)
-    q_wide = q_rows.astype(f32)
-
-    f_q, f_k = (q_wide * jnp.exp(f_cum)).astype(bf16), (f_key * jnp.exp(-f_cum)).astype(bf16)
-    b_q, b_k = (q_wide * jnp.exp(b_cum)).astype(bf16), (b_key * jnp.exp(-b_cum)).astype(bf16)
-    logs = jnp.stack([f_cum[-1], b_cum[0]])
-
-    def digest(keys, log):
-        parts = [
-            lax.dot_general(
-                v_rows[:, h * VAL_DIM : (h + 1) * VAL_DIM],
-                keys[:, h * KEY_DIM : (h + 1) * KEY_DIM],
-                (((0,), (0,)), ((), ())),
-                preferred_element_type=f32,
-            )
-            for h in range(chain_heads)
-        ]
-        return (jnp.concatenate(parts, axis=1) * jnp.exp(log)).astype(bf16)
 
     heads = query_up.shape[1] // ATT_QK
     half = ROPE_DIM // 2
-    inverse = rope_theta ** (-jnp.arange(0, ROPE_DIM, 2).astype(f32) / ROPE_DIM)
-    angles = jnp.arange(seq_len, dtype=jnp.int32).astype(f32)[:, None] * inverse
-    cosine = jnp.tile(jnp.cos(angles), (1, 2))
-    sine = jnp.tile(jnp.sin(angles), (1, 2))
-
-    def tables(gain, cos_rows, sin_rows):
+    inverse = rope_theta ** (-np.arange(0, ROPE_DIM, 2).astype(np.float32) / ROPE_DIM)
+    angles = np.arange(seq_len, dtype=np.float32)[:, None] * inverse.astype(np.float32)
+    cosine, sine = (
+        jnp.asarray(np.tile(turn(angles), (1, 2)).reshape(n_sp, rows, ROPE_DIM), f32)
+        for turn in (np.cos, np.sin)
+    )
+
+    def tails(gain):
         tail = gain[NOPE_DIM:]
-        return cos_rows * tail, sin_rows * jnp.roll(tail, half)
-
-    own_rows = functools.partial(
-        lax.dynamic_slice_in_dim, start_index=sp * rows, slice_size=rows, axis=0
-    )
-    query_tables = tables(query_head_gain, own_rows(cosine), own_rows(sine))
-    key_tables = [
-        t.reshape(n_sp, rows, ROPE_DIM) for t in tables(key_head_gain, cosine, sine)
-    ]
+        return jnp.stack([tail, jnp.roll(tail, half)])
+
     swap = np.zeros((ROPE_DIM, ROPE_DIM), np.float32)
     for j in range(half):
         swap[half + j, j] = -1.0
@@ -671,7 +704,7 @@
         n_tp,
         raw_q,
         raw_l,
-        (logs, digest(f_k, logs[0]), digest(b_k, logs[1]), chain_out, attend_out),
+        (logs, f_state, b_state, chain_out, attend_out),
         (
             f_q,
             f_k,
@@ -682,13 +715,15 @@
             chain_gain[None],
             query_latent_gain.reshape(n_tp, 1, q_cols),
             latent_gain[None],
-            query_up.reshape(n_tp, q_cols, -1),
+            query_up,
             latent_up,
             query_head_gain[None, :NOPE_DIM],
             key_head_gain[None, :NOPE_DIM],
             mixer_gain[None],
-            *query_tables,
-            *key_tables,
+            tails(query_head_gain),
+            tails(key_head_gain),
+            cosine,
+            sine,
             *picks,
         ),
         heads,

time: 146 us -> 135 us (0.925)
  other arithmetic: 6.31 us -> 1.99 us
  matrix products: 3.22 us -> 0 us
  local copies, waits for them, and re-layouts: 9.43 us -> 6.31 us
    dot_general x6 -> x0, matrix products: 3.22 us -> none  [the longest x1 1.33 us: on_device(): f_cum = jnp.dot(lower, f_log, precision=lax.Precision.HIGHEST)]
    mul x3 -> x0, other arithmetic: 2.49 us -> none  [tables(): return (cos_rows * tail, sin_rows * jnp.roll(tail, half))]
    convert_element_type x4 -> x0, other arithmetic: 1.51 us -> none  [the longest x2 1.28 us: digest(): return (jnp.concatenate(parts, axis=1) * jnp.exp(log)).astype(bf16)]
where the time goes in v4:
time: 135 us
  Pallas kernels  127 us (94%)
  local copies, waits for them, and re-layouts  6.31 us (5%)
  other arithmetic  1.99 us (1%)
    pallas_call x1, Pallas kernels, mix_all(): pl.pallas_call(functools.partial(mixer_kernel, n, heads_n), out_shape=jax...  65.3 us
    pallas_call x1, Pallas kernels, project_all(): pl.pallas_call(functools.partial(project_kernel, n, count), out_shape=[ja...  61.5 us

profile of v4, /device:TPU:1, one launch (start us, length us, event | category | flops | bytes accessed | tf_op | source)
XLA Modules:
  0.0 135.1 jit_solution(6521789504058582405)
XLA Ops:
  0.0 0.0 copy-start
  0.0 0.0 copy-start.3
  0.0 0.0 copy-start.2
  0.0 0.7 copy-done.3
  0.7 0.0 copy-done.2
  0.7 0.6 slice_bitcast_fusion.2
  1.3 0.1 fusion.1
  1.4 0.1 maximum_bitcast_fusion
  1.5 0.6 pad_maximum_fusion.1.refs_21_
  2.1 0.1 fusion
  2.1 0.0 copy-start.1
  2.1 0.1 maximum_bitcast_fusion.1
  2.2 0.6 pad_maximum_fusion.2.refs_22_
  2.8 0.0 copy-done.1
  2.8 0.7 reshape.3.refs_14_
  3.5 0.0 dynamic-slice-start
  3.5 0.7 dynamic-slice-done
  4.2 0.1 copy.30
  4.3 0.8 constant_dynamic-slice_fusion
  5.2 0.7 pad_maximum_fusion.refs_9_
  5.8 0.0 copy-done
  5.8 0.8 constant_dynamic-slice_fusion.1.refs_8_
  6.6 61.5 %shard_map.262 = (bf16[160,256]{1,0:T(8,128)(2,1)}, bf16[160,256]{1,0:T(8,128)(2,1)}, bf16[160,192]{1,0:T(8,128)(2,1)}, bf16[160,144]{1,0:T(8,128)(2,1)}, bf16[1...) custom-call(bf16[160,2048]{1,0:T(8,128)(2,1)} %refs_0_.1, ...), custom_call_target="tpu_custom_call" | custom-call | tf_op jit(solution)/shard_map/pallas_call | solution.py:224
  68.1 65.3 %shard_map.263 = f32[40,2048]{1,0:T(8,128)} custom-call(bf16[160,192]{1,0:T(8,128)(2,1)} %get-tuple-element.16.refs_0_, bf16[160,144]{1,0:T(8,128)(2,1)} %get-tuple-element.17.refs_1_, f32[2,256]{1,0:T(2,128)} %get-tuple-element.18.refs_2_, bf16[128,256]{1,0:T(8,128)(2,1)} %get-tuple-element.19.refs_3_, bf16[128,256]{1,0:T(8,128)(2,1)} %get-tuple-element.20.refs_4_, ...), custom_call_target="tpu_custom_call" | custom-call | tf_op jit(solution)/shard_map/pallas_call | solution.py:598
  133.4 1.7 %copy.32 = f32[40,2048]{1,0:T(8,128)} copy(f32[40,2048]{1,0:T(8,128)} %shard_map.263) | data formatting | bytes 655360
Async XLA Ops:
  0.0 5.8 %copy-start = (bf16[256,768]{1,0:T(8,128)(2,1)S(1)}, bf16[256,768]{1,0:T(8,128)(2,1)}, u32[]{:S(2)}) copy-start(bf16[256,768]{1,0:T(8,128)(2,1)} %param.37) | copy-start | bytes 1179652
  0.0 0.7 copy-start.3
  0.0 0.7 copy-start.2
  2.1 0.7 copy-start.1
  3.5 0.7 dynamic-slice-start

commit v5 on v4

--- a/solution.py
+++ b/solution.py
@@ -114,7 +114,8 @@
         )
 
     w_copy(0, 0).start()
-    w_copy(0, 1).start()
+    for c in range(3):
+        w_copy(c, 1).start()
     wide = tokens_ref[...].astype(f32)
     scale = lax.rsqrt(jnp.mean(wide * wide, axis=-1, keepdims=True) + norm_eps)
     normed = (wide * scale * gain_ref[...]).astype(bf16)
@@ -130,8 +131,8 @@
     for c in range(count):
         w_copy(c, 0).wait_recv()
         w_copy(c, 2).start()
-        if c + 1 < count:
-            w_copy(c + 1, 1).start()
+        if c + 3 < count:
+            w_copy(c + 3, 1).start()
     def finished(c):
         def add(d, total):
             p_copy(c, d).wait_recv()

time: 135 us -> 135 us (level)
  no operation moved by 1% of the time
where the time goes in v5:
time: 135 us
  Pallas kernels  127 us (94%)
  local copies, waits for them, and re-layouts  6.31 us (5%)
  other arithmetic  1.99 us (1%)
    pallas_call x1, Pallas kernels, mix_all(): pl.pallas_call(functools.partial(mixer_kernel, n, heads_n), out_shape=jax...  65.3 us
    pallas_call x1, Pallas kernels, project_all(): pl.pallas_call(functools.partial(project_kernel, n, count), out_shape=[ja...  61.5 us

profile of v5, /device:TPU:1, one launch (start us, length us, event | category | flops | bytes accessed | tf_op | source)
XLA Modules:
  0.0 135.1 jit_solution(4819043528035887216)
XLA Ops:
  0.0 0.0 copy-start
  0.0 0.0 copy-start.3
  0.0 0.0 copy-start.2
  0.0 0.7 copy-done.3
  0.7 0.0 copy-done.2
  0.7 0.6 slice_bitcast_fusion.2
  1.3 0.1 fusion.1
  1.4 0.1 maximum_bitcast_fusion
  1.5 0.6 pad_maximum_fusion.1.refs_21_
  2.1 0.1 fusion
  2.1 0.0 copy-start.1
  2.1 0.1 maximum_bitcast_fusion.1
  2.2 0.6 pad_maximum_fusion.2.refs_22_
  2.8 0.0 copy-done.1
  2.8 0.7 reshape.3.refs_14_
  3.5 0.0 dynamic-slice-start
  3.5 0.7 dynamic-slice-done
  4.2 0.1 copy.30
  4.3 0.8 constant_dynamic-slice_fusion
  5.2 0.7 pad_maximum_fusion.refs_9_
  5.8 0.0 copy-done
  5.8 0.8 constant_dynamic-slice_fusion.1.refs_8_
  6.6 61.5 %shard_map.262 = (bf16[160,256]{1,0:T(8,128)(2,1)}, bf16[160,256]{1,0:T(8,128)(2,1)}, bf16[160,192]{1,0:T(8,128)(2,1)}, bf16[160,144]{1,0:T(8,128)(2,1)}, bf16[1...) custom-call(bf16[160,2048]{1,0:T(8,128)(2,1)} %refs_0_.1, ...), custom_call_target="tpu_custom_call" | custom-call | tf_op jit(solution)/shard_map/pallas_call | solution.py:225
  68.1 65.3 %shard_map.263 = f32[40,2048]{1,0:T(8,128)} custom-call(bf16[160,192]{1,0:T(8,128)(2,1)} %get-tuple-element.16.refs_0_, bf16[160,144]{1,0:T(8,128)(2,1)} %get-tuple-element.17.refs_1_, f32[2,256]{1,0:T(2,128)} %get-tuple-element.18.refs_2_, bf16[128,256]{1,0:T(8,128)(2,1)} %get-tuple-element.19.refs_3_, bf16[128,256]{1,0:T(8,128)(2,1)} %get-tuple-element.20.refs_4_, ...), custom_call_target="tpu_custom_call" | custom-call | tf_op jit(solution)/shard_map/pallas_call | solution.py:599
  133.4 1.7 %copy.32 = f32[40,2048]{1,0:T(8,128)} copy(f32[40,2048]{1,0:T(8,128)} %shard_map.263) | data formatting | bytes 655360
Async XLA Ops:
  0.0 5.8 %copy-start = (bf16[256,768]{1,0:T(8,128)(2,1)S(1)}, bf16[256,768]{1,0:T(8,128)(2,1)}, u32[]{:S(2)}) copy-start(bf16[256,768]{1,0:T(8,128)(2,1)} %param.37) | copy-start | bytes 1179652
  0.0 0.7 copy-start.3
  0.0 0.7 copy-start.2
  2.1 0.7 copy-start.1
  3.5 0.7 dynamic-slice-start
